TPU v7x, 32 devices: a whole 2x2x4 slice. The times are simulated.
32 devices in a mesh: st: 4 (over y, x), tp: 8 (over z, core).
Axes of the slice: x: 2, y: 2, z: 4, core: 2. Of those that a mesh axis runs over, the one named last changes fastest.
Arguments:
- tokens: bfloat16 [2048, 4096], P('st', 'tp'), may hold values from -6 to 6
- w_query: bfloat16 [4096, 2048], P(None, 'tp'), may hold values from -0.09375 to 0.09375
- w_key: bfloat16 [4096, 2048], P(None, 'tp'), may hold values from -0.09375 to 0.09375
- w_value: bfloat16 [4096, 4096], P(None, 'tp'), may hold values from -0.09375 to 0.09375
- w_mem_query: bfloat16 [4096, 2048], P(None, 'tp'), may hold values from -0.09375 to 0.09375
- w_mem_key: bfloat16 [4096, 2048], P(None, 'tp'), may hold values from -0.09375 to 0.09375
- w_mem_value: bfloat16 [4096, 2048], P(None, 'tp'), may hold values from -0.09375 to 0.09375
- w_gate: bfloat16 [4096, 16], P(None, 'tp'), may hold values from -0.09375 to 0.09375
- w_lift: bfloat16 [16, 128, 256], P('tp'), may hold values from -4 to 4
- decay_rate: float32 [16], P('tp'), may hold values from 0.000390625 to 0.1
- store: bfloat16 [512, 64, 4096], P('st', None, 'tp'), may hold values from -6 to 6
- passage_ids: int32 [16, 2], P('st'), may hold values from 0 to 511, as said below
Outputs:
- mixed: bfloat16 [2048, 4096], P('st', 'tp')
Inputs may be any that keep to these rules, and one draw needn't show every extreme that they name: `passage_ids`: passage p is held by index p // 128 of st. Among the requests of the rows of one device along st, at most 4 name passages held by one index of st, and in every draw some index receives exactly 4 of them.
All inputs are finite; a program needn't handle non-finite values.
Results may differ from a plain program's by a relative error of at most 0.0095.
Values may be sent and summed in bfloat16 or wider, within the bound.
A program may use at most 64 MiB of HBM per device.

v0:
```python
import functools

import jax
import jax.numpy as jnp
import numpy as np
from jax import lax
from jax.experimental import pallas as pl
from jax.experimental.pallas import tpu as pltpu
from jax.sharding import PartitionSpec as P

KEY_DIM = 128
VALUE_DIM = 256
MEM_DIM = 128
SEQ_LEN = 512
NORM_EPS = 1e-06
ROPE_BASE = 10000.0
CORES = 2
CHUNK = 128
PIECES = 2
SPLIT = 1
MESH = pl.DeviceIdType.MESH
F32 = jnp.float32
BF16 = jnp.bfloat16


def dot(a, b):
    return jnp.dot(a, b, preferred_element_type=F32)


def dot_nt(a, b):
    return lax.dot_general(a, b, (((1,), (1,)), ((), ())), preferred_element_type=F32)


def kernel(
    n_st, n_tp, cap, picks, held,
    rate_ref, tok_hbm, wq_hbm, wk_hbm, wv_hbm, wm_hbm, wmk_hbm, wmv_hbm, wg_ref, lift_hbm,
    cos_hbm, sin_hbm, store_hbm, ids_hbm,
    out_ref,
    tok, rows, cos_ref, sin_ref, lift_ref, wq, wk, wv, wm, wmk, wmv, store, slots, landed, ids_v, ids_s,
    acc_q, acc_k, acc_v, acc_m, acc_g, acc_s, acc_mk, acc_mv,
    rq, rk, rv, mq, ret, gate,
    load_sem, id_send, id_recv, pass_send, pass_recv,
    t_recv, t_send, t_left, t_pair, r_recv, r_send, r_left, r_pair,
):
    st = lax.axis_index("st")
    me = lax.axis_index("tp")
    z = me // CORES
    core = me % CORES
    n_z = n_tp // CORES
    total, cols = tok.shape[1:]
    heads = mq.shape[1] // MEM_DIM
    requests = ids_s.shape[1] * ids_s.shape[2]
    pass_rows = store.shape[1]

    loads = []
    pairs = [(store_hbm, store), (ids_hbm, ids_v.at[st]), (tok_hbm, tok.at[me]), (wq_hbm, wq), (wk_hbm, wk),
             (wv_hbm, wv), (wm_hbm, wm), (wmk_hbm, wmk), (wmv_hbm, wmv),
             (cos_hbm, cos_ref), (sin_hbm, sin_ref), (lift_hbm, lift_ref)]
    for i, (src, dst) in enumerate(pairs):
        loads.append(pltpu.make_async_copy(src, dst, load_sem.at[i]))
    loads[1].start()

    barrier = pltpu.get_barrier_semaphore()
    has_right = z < n_z - 1
    has_left = z > 0

    @pl.when(has_right)
    def _():
        pl.semaphore_signal(barrier, inc=1, device_id=(st, me + CORES), device_id_type=MESH)

    @pl.when(has_left)
    def _():
        pl.semaphore_signal(barrier, inc=1, device_id=(st, me - CORES), device_id_type=MESH)

    pair = z * CORES + (1 - core)
    pl.semaphore_signal(barrier, inc=1, device_id=(st, pair), device_id_type=MESH)
    for d in range(1, n_st):
        pl.semaphore_signal(barrier, inc=1, device_id=((st + d) % n_st, me), device_id_type=MESH)
    pl.semaphore_wait(barrier, n_st + has_right.astype(jnp.int32) + has_left.astype(jnp.int32))

    def remote(src, dst, send, recv, to_st, to_tp):
        return pltpu.make_async_remote_copy(
            src_ref=src, dst_ref=dst, send_sem=send, recv_sem=recv,
            device_id=(to_st, to_tp), device_id_type=MESH)

    def line(buf, sems):
        recv, send, left, pairing = sems
        size = buf.shape[1] // PIECES

        def piece(j, p):
            return buf.at[j, pl.ds(p * size, size)]

        def own_piece(src, p):
            return piece(me, p) if src is None else src.at[pl.ds(p * size, size)]

        def right_copy(j, p, src=None):
            return remote(piece(j, p) if src is None else src, piece(j, p), send.at[j, p], recv.at[j, p],
                          st, me + CORES)

        def left_copy(j, p, src=None):
            sem = left.at[0, p] if src is not None else send.at[j, p]
            return remote(piece(j, p) if src is None else src, piece(j, p), sem, recv.at[j, p], st, me - CORES)

        def pair_copy(j, p, src=None):
            return remote(piece(j, p) if src is None else src, piece(j, p), pairing.at[j, p], recv.at[j, p], st, pair)

        def send_own(src):
            for p in range(PIECES):
                own = own_piece(src, p)

                @pl.when(has_right)
                def _():
                    right_copy(me, p, own).start()

                @pl.when(has_left)
                def _():
                    left_copy(me, p, own).start()
            for p in range(PIECES):
                pair_copy(me, p, own_piece(src, p)).start()

        def relay(d, p):
            from_left = me - CORES * d
            from_right = me + CORES * d

            @pl.when(from_left >= 0)
            def _():
                pair_copy(from_left, p).wait_recv()

                @pl.when(has_right)
                def _():
                    right_copy(from_left, p).start()
                pair_copy(from_left, p).start()

            @pl.when(from_right < n_tp)
            def _():
                pair_copy(from_right, p).wait_recv()

                @pl.when(has_left)
                def _():
                    left_copy(from_right, p).start()
                pair_copy(from_right, p).start()

        def drain(src):
            def step(q, carry):
                d, p = q // PIECES, q % PIECES
                from_left = me - CORES * d
                from_right = me + CORES * d

                @pl.when(from_left >= 0)
                def _():
                    @pl.when(has_right)
                    def _():
                        right_copy(from_left, p).wait_send()
                    pair_copy(from_left, p).wait_send()

                @pl.when((d > 0) & (from_right < n_tp))
                def _():
                    @pl.when(has_left)
                    def _():
                        left_copy(from_right, p).wait_send()
                    pair_copy(from_right, p).wait_send()
                return carry
            for p in range(PIECES):
                @pl.when(has_left)
                def _():
                    left_copy(me, p, own_piece(src, p)).wait_send()
            lax.fori_loop(0, PIECES * n_z, step, 0)

        def consume(low, high, take, p):
            def step(q, carry):
                d, side, which = q // 4, (q // 2) % 2, q % 2
                at = z + (2 * side - 1) * d
                j = at * CORES + which
                valid = (at >= 0) & (at < n_z) & ((d > 0) | (side == 0))

                @pl.when(valid)
                def _():
                    @pl.when(which != core)
                    def _():
                        pair_copy(j, p).wait_recv()
                    take(j, p)
                return carry
            lax.fori_loop(4 * low, 4 * high, step, 0)

        return send_own, relay, drain, consume

    tok_send, tok_relay, tok_drain, tok_consume = line(tok, (t_recv, t_send, t_left, t_pair))
    row_send, row_relay, row_drain, row_consume = line(rows, (r_recv, r_send, r_left, r_pair))

    def id_copy(d):
        return remote(ids_hbm, ids_v.at[st], id_send.at[d], id_recv.at[st], (st + d) % n_st, me)

    def id_wait(d):
        other = (st + d) % n_st
        return remote(ids_hbm, ids_v.at[other], id_send.at[d], id_recv.at[other], other, me)

    for d in range(1, n_st):
        id_copy(d).start()
    tok_send(tok_hbm)
    loads[0].start()
    loads[2].start()

    for ref in (acc_q, acc_k, acc_v, acc_m, acc_g, acc_s, acc_mk, acc_mv):
        ref[...] = jnp.zeros_like(ref)

    loads[1].wait()
    for d in range(1, n_st):
        id_wait(d).wait_recv()
    to_scalar = pltpu.make_async_copy(ids_v, ids_s, load_sem.at[len(pairs)])
    to_scalar.start()
    to_scalar.wait()
    loads[0].wait()

    def asked(source, k):
        found = jnp.int32(0)
        seen = jnp.int32(0)
        for i in range(requests):
            ident = ids_s[source, i % picks, i // picks]
            mine = (ident // held) == st
            found = jnp.where(mine & (seen == k), ident % held, found)
            seen = seen + mine.astype(jnp.int32)
        return found

    def fill(d, carry):
        source = (st + d) % n_st
        for k in range(cap):
            slots[d, k] = store[asked(source, k)]
        return carry
    lax.fori_loop(1, n_st, fill, 0)

    def pass_copy(d):
        return remote(slots.at[d], landed.at[st], pass_send.at[d], pass_recv.at[st], (st + d) % n_st, me)

    def pass_wait(d):
        other = (st + d) % n_st
        return remote(slots.at[d], landed.at[other], pass_send.at[d], pass_recv.at[other], other, me)

    for d in range(1, n_st):
        pass_copy(d).start()
    for k in range(cap):
        landed[st, k] = store[asked(st, k)]
    for i in range(3, len(pairs)):
        loads[i].start()

    for p in range(PIECES):
        tok_relay(1, p)

    for d in range(1, n_st):
        pass_wait(d).wait_recv()
    for i in range(requests):
        ident = ids_s[st, i % picks, i // picks]
        owner = ident // held
        order = jnp.int32(0)
        for e in range(i):
            order = order + ((ids_s[st, e % picks, e // picks] // held) == owner).astype(jnp.int32)
        rows[me, pl.ds(i * pass_rows, pass_rows), :] = landed[owner, jnp.minimum(order, cap - 1)]
    row_send(None)

    for i in range(2, len(pairs)):
        loads[i].wait()

    def take_tokens(j, p):
        at = pl.ds(pl.multiple_of(j * cols, cols), cols)
        step_rows = total // PIECES // SPLIT

        def part(c, carry):
            here = pl.ds(pl.multiple_of((p * SPLIT + c) * step_rows, step_rows), step_rows)
            x = tok[j, here, :]
            acc_q[here, :] += dot(x, wq[at, :])
            acc_k[here, :] += dot(x, wk[at, :])
            acc_v[here, :] += dot(x, wv[at, :])
            acc_m[here, :] += dot(x, wm[at, :])
            wide = x.astype(F32)
            if heads > 1:
                acc_g[here, :] += dot_nt(x, wg_ref[:, at])
            else:
                acc_g[here, :] += jnp.sum(wide * wg_ref[:, at].astype(F32), axis=1, keepdims=True)
            squares = acc_s[here, :]
            for piece in range(cols // 128):
                slab = wide[:, piece * 128:(piece + 1) * 128]
                squares = squares + slab * slab
            acc_s[here, :] = squares
            return carry
        lax.fori_loop(0, SPLIT, part, 0)

    def token_piece(p, carry):
        tok_consume(0, 2, take_tokens, p)
        return carry
    lax.fori_loop(0, PIECES, token_piece, 0)

    def token_stage(q, carry):
        d, p = q // PIECES, q % PIECES
        tok_relay(d, p)
        tok_consume(d, d + 1, take_tokens, p)
        return carry
    lax.fori_loop(2 * PIECES, n_z * PIECES, token_stage, 0)

    for p in range(PIECES):
        row_relay(1, p)

    def prepare(c, carry):
        here = pl.ds(pl.multiple_of(c * CHUNK, CHUNK), CHUNK)
        scale = lax.rsqrt(jnp.sum(acc_s[here, :], axis=1, keepdims=True) / (n_tp * cols) + NORM_EPS)
        cosine, sine = cos_ref[here, :], sin_ref[here, :]

        def rotate(v):
            return v * cosine + pltpu.roll(v, KEY_DIM // 2, 1) * sine
        for h in range(heads):
            at = slice(h * KEY_DIM, (h + 1) * KEY_DIM)
            rq[here, at] = rotate(acc_q[here, at] * scale).astype(BF16)
            rk[here, at] = (rotate(acc_k[here, at] * scale) * KEY_DIM ** (-0.5)).astype(BF16)
            m = acc_m[here, at]
            mq[here, at] = (m * lax.rsqrt(jnp.mean(m * m, axis=1, keepdims=True) + NORM_EPS)).astype(BF16)
        rv[here, :] = (acc_v[here, :] * scale).astype(BF16)
        gate[here, :] = jax.nn.sigmoid(acc_g[here, :] * scale)
        return carry
    lax.fori_loop(0, total // CHUNK, prepare, 0)

    def retain(c, carry):
        here = pl.ds(pl.multiple_of(c * CHUNK, CHUNK), CHUNK)
        start = (c * CHUNK) // SEQ_LEN * SEQ_LEN
        whole = pl.ds(pl.multiple_of(start, SEQ_LEN), SEQ_LEN)
        t = lax.broadcasted_iota(jnp.int32, (CHUNK, SEQ_LEN), 0) + (c * CHUNK - start)
        s = lax.broadcasted_iota(jnp.int32, (CHUNK, SEQ_LEN), 1)
        gap = (t - s).astype(F32)
        for h in range(heads):
            at = slice(h * KEY_DIM, (h + 1) * KEY_DIM)
            wide = slice(h * VALUE_DIM, (h + 1) * VALUE_DIM)
            decay = jnp.where(gap >= 0.0, jnp.exp(-rate_ref[h] * jnp.maximum(gap, 0.0)), 0.0)
            scores = dot_nt(rq[here, at], rk[whole, at]) * decay
            upper = scores.astype(BF16)
            lower = (scores - upper.astype(F32)).astype(BF16)
            value = rv[whole, wide]
            o = dot(upper, value) + dot(lower, value)
            o = o - jnp.mean(o, axis=1, keepdims=True)
            ret[here, wide] = o * lax.rsqrt(jnp.mean(o * o, axis=1, keepdims=True) + NORM_EPS)
        return carry
    lax.fori_loop(0, total // CHUNK, retain, 0)

    def take_rows(j, p):
        at = pl.ds(pl.multiple_of(j * cols, cols), cols)
        size = rows.shape[1] // PIECES
        here = pl.ds(pl.multiple_of(p * size, size), size)
        x = rows[j, here, :]
        acc_mk[here, :] += dot(x, wmk[at, :])
        acc_mv[here, :] += dot(x, wmv[at, :])

    def row_piece(p, carry):
        row_consume(0, 2, take_rows, p)
        return carry
    lax.fori_loop(0, PIECES, row_piece, 0)

    blocks = requests // picks
    block = total // blocks
    keys = picks * pass_rows

    def attend(b, carry):
        here = pl.ds(pl.multiple_of(b * block, block), block)
        there = pl.ds(pl.multiple_of(b * keys, keys), keys)
        for h in range(heads):
            at = slice(h * MEM_DIM, (h + 1) * MEM_DIM)
            wide = slice(h * VALUE_DIM, (h + 1) * VALUE_DIM)
            k = acc_mk[there, at]
            k = (k * lax.rsqrt(jnp.mean(k * k, axis=1, keepdims=True) + NORM_EPS)).astype(BF16)
            v = acc_mv[there, at].astype(BF16)
            exponent = jnp.exp(dot_nt(mq[here, at], k) * MEM_DIM ** (-0.5))
            mass = jnp.sum(exponent, axis=1, keepdims=True)
            o = (dot(exponent.astype(BF16), v) / mass).astype(BF16)
            lifted = dot(o, lift_ref[h])
            out_ref[here, wide] = (ret[here, wide] + gate[here, h:h + 1] * lifted).astype(BF16)
        return carry
    def row_stage(q, carry):
        d, p = q // PIECES, q % PIECES
        row_relay(d, p)
        row_consume(d, d + 1, take_rows, p)

        @pl.when(d == n_z - 1)
        def _():
            share = blocks // PIECES
            lax.fori_loop(p * share, (p + 1) * share, attend, 0)
        return carry
    lax.fori_loop(2 * PIECES, n_z * PIECES, row_stage, 0)

    for d in range(1, n_st):
        id_copy(d).wait_send()
        pass_copy(d).wait_send()
    tok_drain(tok_hbm)
    row_drain(None)


def rotary_tables(total):
    half = KEY_DIM // 2
    angle = (np.arange(total) % SEQ_LEN)[:, None] * ROPE_BASE ** (-np.arange(half) / half)[None, :]
    cosine, sine = np.cos(angle), np.sin(angle)
    return (np.concatenate([cosine, cosine], 1).astype(np.float32),
            np.concatenate([-sine, sine], 1).astype(np.float32))


def solution(mesh):
    n_st, n_tp = mesh.shape["st"], mesh.shape["tp"]

    def per_device(tokens, w_query, w_key, w_value, w_mem_query, w_mem_key, w_mem_value, w_gate, w_lift,
                   decay_rate, store, passage_ids):
        total, cols = tokens.shape
        heads = decay_rate.shape[0]
        blocks, picks = passage_ids.shape
        requests = blocks * picks
        held, pass_rows, _ = store.shape
        cap = max(1, 2 * requests // n_st)
        cosine, sine = rotary_tables(total)
        hbm = pl.BlockSpec(memory_space=pl.ANY)
        vmem = pl.BlockSpec(memory_space=pltpu.VMEM)
        smem = pl.BlockSpec(memory_space=pltpu.SMEM)
        V = pltpu.VMEM
        dma = pltpu.SemaphoreType.DMA
        wide = w_value.shape[1]
        key_cols, mem_cols = w_query.shape[1], w_mem_query.shape[1]
        scratch = [
            V((n_tp, total, cols), BF16), V((n_tp, requests * pass_rows, cols), BF16),
            V(cosine.shape, F32), V(sine.shape, F32), V(w_lift.shape, BF16),
            V(w_query.shape, BF16), V(w_key.shape, BF16), V(w_value.shape, BF16),
            V(w_mem_query.shape, BF16), V(w_mem_key.shape, BF16), V(w_mem_value.shape, BF16),
            V(store.shape, BF16), V((n_st, cap, pass_rows, cols), BF16), V((n_st, cap, pass_rows, cols), BF16),
            V((n_st, picks, blocks), jnp.int32), pltpu.SMEM((n_st, picks, blocks), jnp.int32),
            V((total, key_cols), F32), V((total, key_cols), F32), V((total, wide), F32), V((total, mem_cols), F32),
            V((total, heads), F32), V((total, 128), F32),
            V((requests * pass_rows, mem_cols), F32), V((requests * pass_rows, mem_cols), F32),
            V((total, key_cols), BF16), V((total, key_cols), BF16), V((total, wide), BF16), V((total, mem_cols), BF16),
            V((total, wide), F32), V((total, heads), F32),
            dma((16,)), dma((n_st,)), dma((n_st,)), dma((n_st,)), dma((n_st,)),
            dma((n_tp, PIECES)), dma((n_tp, PIECES)), dma((1, PIECES)), dma((n_tp, PIECES)),
            dma((n_tp, PIECES)), dma((n_tp, PIECES)), dma((1, PIECES)), dma((n_tp, PIECES)),
        ]
        return pl.pallas_call(
            functools.partial(kernel, n_st, n_tp, cap, picks, held),
            out_shape=jax.ShapeDtypeStruct((total, heads * VALUE_DIM), BF16),
            in_specs=[smem] + [hbm] * 7 + [vmem] + [hbm] * 5,
            out_specs=vmem,
            scratch_shapes=scratch,
            compiler_params=pltpu.CompilerParams(
                collective_id=0, has_side_effects=True, vmem_limit_bytes=60 * 1024 * 1024),
        )(decay_rate, tokens, w_query, w_key, w_value, w_mem_query, w_mem_key, w_mem_value,
          w_gate.T, w_lift, jnp.asarray(cosine), jnp.asarray(sine), store, passage_ids.T)

    in_specs = (P("st", "tp"),) + (P(None, "tp"),) * 7 + (
        P("tp", None, None), P("tp"), P("st", None, "tp"), P("st", None))
    return jax.shard_map(per_device, mesh=mesh, in_specs=in_specs, out_specs=P("st", "tp"), check_vma=False)
```

profile of v0, /device:TPU:0, one launch (start us, length us, event | category | flops | bytes accessed | tf_op | source)
XLA Modules:
  0.0 80.9 jit_solution(13810576936190177473)
XLA Ops:
  0.0 79.0 %shard_map.136 = bf16[512,512]{1,0:T(8,128)(2,1)} custom-call(f32[2]{0:T(128)} %rate_ref.1, bf16[512,512]{1,0:T(8,128)(2,1)} %tok_hbm.1, bf16[4096,256]{1,0:T(8,128)(2,1)} %wq_hbm.1, bf16[4096,256]{1,0:T(8,128)(2,1)} %wk_hbm.1, bf16[4096,512]{1,0:T(8,128)(2,1)} %wv_hbm.1, bf16[4096,256]{1,0:T(8,128)(2,1)} %wm_hbm.1, bf16[4096,256]{1,0:T(8,128)(2,1)} %wmk_hbm.1, ...), custom_call_target="tpu_custom_call" | custom-call | tf_op jit(solution)/shard_map/pallas_call | solution.py:434
  79.0 1.9 %copy.16 = bf16[512,512]{1,0:T(8,128)(2,1)} copy(bf16[512,512]{1,0:T(8,128)(2,1)} %shard_map.136) | data formatting | bytes 1048576
where the time goes:
time: 82.1 us; the launch traced here: 80.9 us
  Pallas kernels  79 us (96%)
  local copies, waits for them, and re-layouts  1.87 us (2%)
    pallas_call x1, Pallas kernels, per_device(): pl.pallas_call(functools.partial(kernel, n_st, n_tp, cap, picks, held), o...  79 us
    unnamed x1, local copies, waits for them, and re-layouts  1.87 us

commit v1 on v0

v1 whole, which is shorter than its diff:
```python
import functools

import jax
import jax.numpy as jnp
import numpy as np
from jax import lax
from jax.experimental import pallas as pl
from jax.experimental.pallas import tpu as pltpu
from jax.sharding import PartitionSpec as P

KEY_DIM = 128
VALUE_DIM = 256
MEM_DIM = 128
SEQ_LEN = 512
NORM_EPS = 1e-06
ROPE_BASE = 10000.0
CORES = 2
PIECES = 4
OUT, IN = 0, 1
MESH = pl.DeviceIdType.MESH
F32 = jnp.float32
BF16 = jnp.bfloat16


def dot(a, b):
    return jnp.dot(a, b, preferred_element_type=F32)


def dot_nt(a, b):
    return lax.dot_general(a, b, (((1,), (1,)), ((), ())), preferred_element_type=F32)


def square_split(n):
    return 1 << ((n.bit_length() - 1) // 2)


def kernel(
    n_st, n_tp, cap, picks, held,
    rate_ref, tok_hbm, wq_hbm, wk_hbm, wv_hbm, wm_hbm, wmk_hbm, wmv_hbm, wg_ref, lift_hbm,
    cos_hbm, sin_hbm, store_hbm, ids_hbm,
    out_ref,
    tok, rows, cos_ref, sin_ref, lift_ref, wq, wk, wv, wm, wmk, wmv, store, slots, landed, ids_v, ids_s,
    acc_q, acc_k, acc_v, acc_m, acc_g, acc_s, acc_mk, acc_mv,
    rq, rk, rv, mq, ret, gate, xwk, xwv, kv_out, kv_in,
    load_sem, id_send, id_recv, pass_send, pass_recv,
    t_sems, r_sems, w_send, w_recv, spread_send, kv_send, kv_recv,
):
    st = lax.axis_index("st")
    me = lax.axis_index("tp")
    z = me // CORES
    core = me % CORES
    n_z = n_tp // CORES
    total, cols = tok.shape[1:]
    heads = mq.shape[1] // MEM_DIM
    mem_cols = mq.shape[1]
    requests = ids_s.shape[1] * ids_s.shape[2]
    blocks = requests // picks
    pass_rows = store.shape[1]
    parts = len(landed)
    per = cap // parts
    chunk = total // PIECES
    rows_piece = rows.shape[1] // PIECES

    so = jnp.where(z < n_z // 2, -1, 1)
    depth = jnp.minimum(z, n_z - 1 - z)
    edge_z = z + so * depth
    is_edge = depth == 0
    is_helper = depth == 1
    me_out = me + CORES * so
    me_in = me - CORES * so
    pair = me + 1 - 2 * core
    outs = range(1, (n_z - 1) // 2 + 1)
    ins = range(1, n_z)

    loads = []
    pairs = [(store_hbm, store), (ids_hbm, ids_v.at[st]), (tok_hbm, tok.at[me]), (wq_hbm, wq), (wk_hbm, wk),
             (wv_hbm, wv), (wm_hbm, wm), (wmk_hbm, wmk), (wmv_hbm, wmv),
             (cos_hbm, cos_ref), (sin_hbm, sin_ref), (lift_hbm, lift_ref)]
    for i, (src, dst) in enumerate(pairs):
        loads.append(pltpu.make_async_copy(src, dst, load_sem.at[i]))
    loads[1].start()

    barrier = pltpu.get_barrier_semaphore()

    def greet(to_st, to_tp):
        pl.semaphore_signal(barrier, inc=1, device_id=(to_st, to_tp), device_id_type=MESH)

    @pl.when(depth > 0)
    def _():
        greet(st, me_out)
    greet(st, me_in)
    greet(st, pair)
    for d in range(1, n_st):
        greet((st + d) % n_st, me)
    pl.semaphore_wait(barrier, n_st + 1 + (depth > 0).astype(jnp.int32))

    def remote(src, dst, send, recv, to_st, to_tp):
        return pltpu.make_async_remote_copy(
            src_ref=src, dst_ref=dst, send_sem=send, recv_sem=recv,
            device_id=(to_st, to_tp), device_id_type=MESH)

    class Flow:
        def __init__(self, buf, sems, floor, source=None):
            self.buf, self.floor, self.source = buf, floor, source
            self.recv, self.send, self.own_out, self.pairing = sems
            self.size = buf.shape[1] // PIECES

        def piece(self, j, p):
            return self.buf.at[j, pl.ds(p * self.size, self.size)]

        def origin(self, p):
            return self.piece(me, p) if self.source is None else self.source.at[pl.ds(p * self.size, self.size)]

        def copy(self, j, p, sem, to, src=None):
            return remote(self.piece(j, p) if src is None else src, self.piece(j, p), sem, self.recv.at[j, p], st, to)

        def to_in(self, j, p, src=None):
            return self.copy(j, p, self.send.at[j, p], me_in, src)

        def to_out(self, j, p, src=None):
            return self.copy(j, p, self.send.at[j, p] if src is None else self.own_out.at[p], me_out, src)

        def to_pair(self, j, p, src=None):
            return self.copy(j, p, self.pairing.at[j, p], pair, src)

        def send_own(self, p):
            self.to_in(me, p, self.origin(p)).start()

            @pl.when(depth > self.floor)
            def _():
                self.to_out(me, p, self.origin(p)).start()

        def share_own(self, p):
            self.to_pair(me, p, self.origin(p)).start()

        def at(self, side, d):
            far = CORES * so * d
            if side == OUT:
                return me + far, d <= depth
            return me - far, (d <= n_z - 1 - depth) & (depth >= self.floor)

        def relay(self, side, d, p):
            j, valid = self.at(side, d)

            @pl.when(valid)
            def _():
                self.to_pair(j, p).wait_recv()
                if side == OUT:
                    self.to_in(j, p).start()
                else:
                    @pl.when(depth > self.floor)
                    def _():
                        self.to_out(j, p).start()
                self.to_pair(j, p).start()

        def consume(self, side, d, first, last, take):
            j, valid = self.at(side, d)

            def step(q, carry):
                p, which = first + q // CORES, q % CORES
                this = j + which * (1 - 2 * core)

                @pl.when(which == 1)
                def _():
                    self.to_pair(this, p).wait_recv()
                take(this, p)
                return carry

            if d == 0:
                lax.fori_loop(0, CORES * (last - first), step, 0)
            else:
                @pl.when(valid)
                def _():
                    lax.fori_loop(0, CORES * (last - first), step, 0)

        def drain(self):
            def step(p, carry):
                self.to_in(me, p, self.origin(p)).wait_send()
                self.to_pair(me, p, self.origin(p)).wait_send()

                @pl.when(depth > self.floor)
                def _():
                    self.to_out(me, p, self.origin(p)).wait_send()
                for side, distances in ((OUT, outs), (IN, ins)):
                    for d in distances:
                        j, valid = self.at(side, d)

                        @pl.when(valid)
                        def _():
                            if side == OUT:
                                self.to_in(j, p).wait_send()
                            else:
                                @pl.when(depth > self.floor)
                                def _():
                                    self.to_out(j, p).wait_send()
                            self.to_pair(j, p).wait_send()
                return carry
            lax.fori_loop(0, PIECES, step, 0)

    toks = Flow(tok, t_sems, 0, tok_hbm)
    passes = Flow(rows, r_sems, 1)

    n_b = square_split(n_st)
    n_a = n_st // n_b
    a, b = st // n_b, st % n_b
    row_mates = [a * n_b + (b + i) % n_b for i in range(1, n_b)]
    col_mates = [(a + i) % n_a * n_b + b for i in range(1, n_a)]
    mates = row_mates + col_mates
    along_row = range(0, n_b - 1)
    along_col = range(n_b - 1, len(mates))
    sub = CORES * cols // n_st
    lent = 2 * (n_z - 1)
    xw = (xwk, xwv)

    def lent_at(e, s):
        return pl.ds(pl.multiple_of((edge_z - so * (e + 1)) * (CORES * cols) + s * sub, sub), sub)

    def lend(w):
        kv, e = w % 2, w // 2
        at = lent_at(e, st)
        return remote((wmk_hbm, wmv_hbm)[kv].at[at], xw[kv].at[at], w_send.at[kv, e], w_recv.at[kv, e, st], st, me_in)

    def spread(kv, e, s, i):
        here = xw[kv].at[lent_at(e, s)]
        return remote(here, here, spread_send.at[kv, i, s], w_recv.at[kv, e, s], mates[i], me)

    def spread_own(w):
        kv, e = w % 2, w // 2

        @pl.when(is_helper)
        def _():
            spread(kv, e, st, 0).wait_recv()
            for i in range(len(mates)):
                spread(kv, e, st, i).start()

    def spread_on(w):
        kv, e = w % 2, w // 2

        @pl.when(is_helper)
        def _():
            for s in (row_mates, col_mates)[kv]:
                spread(kv, e, s, 0).wait_recv()
                for i in (along_col, along_row)[kv]:
                    spread(kv, e, s, i).start()

    def spread_last(w):
        kv, e = w % 2, w // 2

        @pl.when(is_helper)
        def _():
            if kv == 0:
                rest = [(a + i) % n_a * n_b + k for i in range(1, n_a) for k in range(n_b)]
            else:
                rest = [k * n_b + (b + i) % n_b for i in range(1, n_b) for k in range(n_a)]
            for s in rest:
                spread(kv, e, s, 0).wait_recv()

    def spread_drain():
        def all_of(kv, s, i):
            whole = xw[kv].at[pl.ds(0, (n_z - 1) * sub)]
            return remote(whole, whole, spread_send.at[kv, i, s], w_recv.at[kv, 0, s], mates[i], me)

        @pl.when(is_helper)
        def _():
            for kv in range(2):
                for i in range(len(mates)):
                    all_of(kv, st, i).wait_send()
                for s in (row_mates, col_mates)[kv]:
                    for i in (along_col, along_row)[kv]:
                        all_of(kv, s, i).wait_send()

        @pl.when(is_edge)
        def _():
            for w in range(lent):
                lend(w).wait_send()

    def kv_copy(p):
        at = pl.ds(p * rows_piece, rows_piece)
        return remote(kv_out.at[at], kv_in.at[at], kv_send.at[p], kv_recv.at[p], st, me_out)

    def id_copy(d):
        return remote(ids_hbm, ids_v.at[st], id_send.at[d], id_recv.at[st], (st + d) % n_st, me)

    def id_wait(d):
        other = (st + d) % n_st
        return remote(ids_hbm, ids_v.at[other], id_send.at[d], id_recv.at[other], other, me)

    half = PIECES // 2
    late = lent - 2
    for d in range(1, n_st):
        id_copy(d).start()
    for p in range(half):
        @pl.when(is_edge)
        def _():
            lend(p).start()
        toks.send_own(p)

    @pl.when(is_edge)
    def _():
        for w in range(half, late):
            lend(w).start()

    @pl.when(depth > 0)
    def _():
        for p in range(half, PIECES):
            toks.send_own(p)
    loads[0].start()
    for p in range(PIECES):
        toks.share_own(p)
    loads[2].start()

    for ref in (acc_q, acc_k, acc_v, acc_m, acc_g, acc_s, acc_mk, acc_mv):
        ref[...] = jnp.zeros_like(ref)

    loads[1].wait()
    for d in range(1, n_st):
        id_wait(d).wait_recv()
    to_scalar = pltpu.make_async_copy(ids_v, ids_s, load_sem.at[len(pairs)])
    to_scalar.start()
    to_scalar.wait()
    loads[0].wait()

    def asked(source, k):
        found = jnp.int32(0)
        seen = jnp.int32(0)
        for i in range(requests):
            ident = ids_s[source, i % picks, i // picks]
            mine = (ident // held) == st
            found = jnp.where(mine & (seen == k), ident % held, found)
            seen = seen + mine.astype(jnp.int32)
        return found

    def pass_copy(g, d):
        return remote(slots.at[d, pl.ds(g * per, per)], landed[g].at[st], pass_send.at[g, d], pass_recv.at[g, st],
                      (st + d) % n_st, me)

    def pass_wait(g, d):
        other = (st + d) % n_st
        return remote(slots.at[d, pl.ds(g * per, per)], landed[g].at[other], pass_send.at[g, d],
                      pass_recv.at[g, other], other, me)

    for g in range(parts):
        def fill(d, carry):
            for k in range(g * per, (g + 1) * per):
                slots[d, k] = store[asked((st + d) % n_st, k)]
            return carry
        lax.fori_loop(1, n_st, fill, 0)
        for d in range(1, n_st):
            pass_copy(g, d).start()
    for k in range(cap):
        landed[k // per][st, k % per] = store[asked(st, k)]
    for i in range(3, len(pairs)):
        loads[i].start()

    def build(block):
        reach = min(parts, -(-picks * (block + 1) // per))
        for i in range(block * picks, (block + 1) * picks):
            ident = ids_s[st, i % picks, i // picks]
            owner = ident // held
            order = jnp.int32(0)
            for e in range(i):
                order = order + ((ids_s[st, e % picks, e // picks] // held) == owner).astype(jnp.int32)
            value = landed[0][owner, jnp.minimum(order, per - 1)]
            for g in range(1, reach):
                other = landed[g][owner, jnp.clip(order - g * per, 0, per - 1)]
                value = jnp.where(order >= g * per, other, value)
            rows[me, pl.ds(i * pass_rows, pass_rows), :] = value

    def build_piece(p):
        for block in range(p * blocks // PIECES, (p + 1) * blocks // PIECES):
            build(block)

    def take_tokens(j, p):
        at = pl.ds(pl.multiple_of(j * cols, cols), cols)
        here = pl.ds(pl.multiple_of(p * chunk, chunk), chunk)
        x = tok[j, here, :]
        acc_q[here, :] += dot(x, wq[at, :])
        acc_k[here, :] += dot(x, wk[at, :])
        acc_v[here, :] += dot(x, wv[at, :])
        acc_m[here, :] += dot(x, wm[at, :])
        wide = x.astype(F32)
        if heads > 1:
            acc_g[here, :] += dot_nt(x, wg_ref[:, at])
        else:
            acc_g[here, :] += jnp.sum(wide * wg_ref[:, at].astype(F32), axis=1, keepdims=True)
        squares = acc_s[here, :]
        for piece in range(cols // 128):
            slab = wide[:, piece * 128:(piece + 1) * 128]
            squares = squares + slab * slab
        acc_s[here, :] = squares

    def take_rows(j, p):
        at = pl.ds(pl.multiple_of(j * cols, cols), cols)
        here = pl.ds(pl.multiple_of(p * rows_piece, rows_piece), rows_piece)
        x = rows[j, here, :]
        acc_mk[here, :] += dot(x, wmk[at, :])
        acc_mv[here, :] += dot(x, wmv[at, :])

    def prepare(c, carry):
        here = pl.ds(pl.multiple_of(c * chunk, chunk), chunk)
        scale = lax.rsqrt(jnp.sum(acc_s[here, :], axis=1, keepdims=True) / (n_tp * cols) + NORM_EPS)
        cosine, sine = cos_ref[here, :], sin_ref[here, :]

        def rotate(v):
            return v * cosine + pltpu.roll(v, KEY_DIM // 2, 1) * sine
        for h in range(heads):
            at = slice(h * KEY_DIM, (h + 1) * KEY_DIM)
            rq[here, at] = rotate(acc_q[here, at] * scale).astype(BF16)
            rk[here, at] = (rotate(acc_k[here, at] * scale) * KEY_DIM ** (-0.5)).astype(BF16)
            m = acc_m[here, at]
            mq[here, at] = (m * lax.rsqrt(jnp.mean(m * m, axis=1, keepdims=True) + NORM_EPS)).astype(BF16)
        rv[here, :] = (acc_v[here, :] * scale).astype(BF16)
        gate[here, :] = jax.nn.sigmoid(acc_g[here, :] * scale)
        return carry

    def retain(c):
        here = pl.ds(c * chunk, chunk)
        start = (c * chunk) // SEQ_LEN * SEQ_LEN
        length = (c + 1) * chunk - start
        whole = pl.ds(start, length)
        t = lax.broadcasted_iota(jnp.int32, (chunk, length), 0) + (c * chunk - start)
        s = lax.broadcasted_iota(jnp.int32, (chunk, length), 1)
        gap = (t - s).astype(F32)
        for h in range(heads):
            at = slice(h * KEY_DIM, (h + 1) * KEY_DIM)
            wide = slice(h * VALUE_DIM, (h + 1) * VALUE_DIM)
            decay = jnp.where(gap >= 0.0, jnp.exp(-rate_ref[h] * jnp.maximum(gap, 0.0)), 0.0)
            scores = dot_nt(rq[here, at], rk[whole, at]) * decay
            upper = scores.astype(BF16)
            lower = (scores - upper.astype(F32)).astype(BF16)
            value = rv[whole, wide]
            o = dot(upper, value) + dot(lower, value)
            o = o - jnp.mean(o, axis=1, keepdims=True)
            ret[here, wide] = o * lax.rsqrt(jnp.mean(o * o, axis=1, keepdims=True) + NORM_EPS)

    def assist(p):
        @pl.when(is_helper)
        def _():
            at = pl.ds(pl.multiple_of(p * rows_piece, rows_piece), rows_piece)
            base = jnp.where(so < 0, CORES, 0)
            for kv in range(2):
                total_kv = None
                for q in range(CORES * (n_z - 1)):
                    j = base + q
                    part = dot(rows[j, at, :], xw[kv][pl.ds(pl.multiple_of(j * cols, cols), cols), :])
                    total_kv = part if total_kv is None else total_kv + part
                kv_out[at, kv * mem_cols:(kv + 1) * mem_cols] = total_kv.astype(BF16)
            kv_copy(p).start()

    block = total // blocks
    keys = picks * pass_rows

    def attend(n, carry):
        here = pl.ds(pl.multiple_of(n * block, block), block)
        there = pl.ds(pl.multiple_of(n * keys, keys), keys)
        for h in range(heads):
            at = slice(h * MEM_DIM, (h + 1) * MEM_DIM)
            wide = slice(h * VALUE_DIM, (h + 1) * VALUE_DIM)
            k = acc_mk[there, at]
            k = (k * lax.rsqrt(jnp.mean(k * k, axis=1, keepdims=True) + NORM_EPS)).astype(BF16)
            v = acc_mv[there, at].astype(BF16)
            exponent = jnp.exp(dot_nt(mq[here, at], k) * MEM_DIM ** (-0.5))
            mass = jnp.sum(exponent, axis=1, keepdims=True)
            o = (dot(exponent.astype(BF16), v) / mass).astype(BF16)
            lifted = dot(o, lift_ref[h])
            out_ref[here, wide] = (ret[here, wide] + gate[here, h:h + 1] * lifted).astype(BF16)
        return carry

    def tokens_of(side, d, first, last):
        toks.consume(side, d, first, last, take_tokens)

    def rows_of(side, d, p):
        passes.consume(side, d, p, p + 1, take_rows)

    for p in range(half):
        toks.relay(IN, 1, p)
        spread_own(p)
        for d in outs:
            toks.relay(OUT, d, p)
    for i in range(2, len(pairs)):
        loads[i].wait()
    tokens_of(IN, 0, 0, PIECES)
    for p in range(half, PIECES):
        toks.relay(IN, 1, p)

    for d in range(1, n_st):
        pass_wait(0, d).wait_recv()
    first_needs = min(parts, -(-picks * (blocks // PIECES) // per))
    for g in range(1, first_needs):
        for d in range(1, n_st):
            pass_wait(g, d).wait_recv()
    build_piece(0)
    passes.send_own(0)
    passes.share_own(0)

    @pl.when(is_edge)
    def _():
        for p in range(half, PIECES):
            toks.send_own(p)
        for w in range(late, lent):
            lend(w).start()

    tokens_of(IN, 1, 0, PIECES)
    for w in range(half, late):
        spread_own(w)
    for p in range(half):
        toks.relay(IN, 2, p)
    for d in outs:
        tokens_of(OUT, d, 0, half)
    tokens_of(IN, 2, 0, half)

    for g in range(first_needs, parts):
        for d in range(1, n_st):
            pass_wait(g, d).wait_recv()
    for p in range(1, PIECES):
        build_piece(p)
        passes.share_own(p)
    passes.send_own(1)

    @pl.when(is_edge)
    def _():
        for p in range(2, PIECES):
            passes.send_own(p)

    for d in outs:
        passes.relay(OUT, d, 0)
    passes.relay(IN, 1, 0)
    for w in range(half):
        spread_on(w)
    for p in range(half, PIECES):
        for d in outs:
            toks.relay(OUT, d, p)

    @pl.when(depth > 0)
    def _():
        for p in range(2, PIECES):
            passes.send_own(p)

    for d in ins[1:]:
        passes.relay(IN, d, 0)
    for p in range(half, PIECES):
        toks.relay(IN, 2, p)
    for d in ins[2:]:
        for p in range(half):
            toks.relay(IN, d, p)
        tokens_of(IN, d, 0, half)
    for c in range(half):
        prepare(c, 0)
        retain(c)
    for w in range(half, late):
        spread_on(w)
    for w in range(late, lent):
        spread_own(w)
    for d in outs:
        tokens_of(OUT, d, half, PIECES)
    tokens_of(IN, 2, half, PIECES)
    for d in ins[2:]:
        for p in range(half, PIECES):
            toks.relay(IN, d, p)
        tokens_of(IN, d, half, PIECES)

    def rows_relay(p):
        for d in outs:
            passes.relay(OUT, d, p)
        for d in ins:
            passes.relay(IN, d, p)

    def rows_take(p):
        rows_of(IN, 0, p)
        for d in outs:
            rows_of(OUT, d, p)
        for d in ins:
            rows_of(IN, d, p)

    rows_relay(1)
    for w in range(late, lent):
        spread_on(w)
    for c in range(half, PIECES):
        prepare(c, 0)
        retain(c)
    for w in range(lent):
        spread_last(w)

    def finish(p, carry):
        @pl.when(p > 1)
        def _():
            rows_relay(p)
        rows_take(p)
        assist(p)

        @pl.when(is_edge)
        def _():
            at = pl.ds(pl.multiple_of(p * rows_piece, rows_piece), rows_piece)
            kv_copy(p).wait_recv()
            acc_mk[at, :] += kv_in[at, :mem_cols].astype(F32)
            acc_mv[at, :] += kv_in[at, mem_cols:].astype(F32)
        share = blocks // PIECES
        lax.fori_loop(p * share, (p + 1) * share, attend, 0)
        return carry
    lax.fori_loop(0, PIECES, finish, 0)

    for d in range(1, n_st):
        id_copy(d).wait_send()
        for g in range(parts):
            pass_copy(g, d).wait_send()
    toks.drain()
    passes.drain()
    spread_drain()

    @pl.when(is_helper)
    def _():
        for p in range(PIECES):
            kv_copy(p).wait_send()


def rotary_tables(total):
    half = KEY_DIM // 2
    angle = (np.arange(total) % SEQ_LEN)[:, None] * ROPE_BASE ** (-np.arange(half) / half)[None, :]
    cosine, sine = np.cos(angle), np.sin(angle)
    return (np.concatenate([cosine, cosine], 1).astype(np.float32),
            np.concatenate([-sine, sine], 1).astype(np.float32))


def solution(mesh):
    n_st, n_tp = mesh.shape["st"], mesh.shape["tp"]
    n_z = n_tp // CORES
    assert n_z >= 4

    def per_device(tokens, w_query, w_key, w_value, w_mem_query, w_mem_key, w_mem_value, w_gate, w_lift,
                   decay_rate, store, passage_ids):
        total, cols = tokens.shape
        heads = decay_rate.shape[0]
        blocks, picks = passage_ids.shape
        requests = blocks * picks
        held, pass_rows, _ = store.shape
        cap = max(1, 2 * requests // n_st)
        parts = cap // picks if cap % picks == 0 else 1
        cosine, sine = rotary_tables(total)
        hbm = pl.BlockSpec(memory_space=pl.ANY)
        vmem = pl.BlockSpec(memory_space=pltpu.VMEM)
        smem = pl.BlockSpec(memory_space=pltpu.SMEM)
        V = pltpu.VMEM
        dma = pltpu.SemaphoreType.DMA
        wide = w_value.shape[1]
        key_cols, mem_cols = w_query.shape[1], w_mem_query.shape[1]
        n_b = square_split(n_st)
        n_mates = n_b - 1 + n_st // n_b - 1

        def flow_sems():
            return dma((n_tp, PIECES)), dma((n_tp, PIECES)), dma((PIECES,)), dma((n_tp, PIECES))
        all_rows = requests * pass_rows
        scratch = [
            V((n_tp, total, cols), BF16), V((n_tp, all_rows, cols), BF16),
            V(cosine.shape, F32), V(sine.shape, F32), V(w_lift.shape, BF16),
            V(w_query.shape, BF16), V(w_key.shape, BF16), V(w_value.shape, BF16),
            V(w_mem_query.shape, BF16), V(w_mem_key.shape, BF16), V(w_mem_value.shape, BF16),
            V(store.shape, BF16), V((n_st, cap, pass_rows, cols), BF16),
            tuple(V((n_st, cap // parts, pass_rows, cols), BF16) for _ in range(parts)),
            V((n_st, picks, blocks), jnp.int32), pltpu.SMEM((n_st, picks, blocks), jnp.int32),
            V((total, key_cols), F32), V((total, key_cols), F32), V((total, wide), F32), V((total, mem_cols), F32),
            V((total, heads), F32), V((total, 128), F32),
            V((all_rows, mem_cols), F32), V((all_rows, mem_cols), F32),
            V((total, key_cols), BF16), V((total, key_cols), BF16), V((total, wide), BF16), V((total, mem_cols), BF16),
            V((total, wide), F32), V((total, heads), F32),
            V(w_mem_key.shape, BF16), V(w_mem_value.shape, BF16),
            V((all_rows, 2 * mem_cols), BF16), V((all_rows, 2 * mem_cols), BF16),
            dma((16,)), dma((n_st,)), dma((n_st,)), dma((parts, n_st)), dma((parts, n_st)),
            flow_sems(), flow_sems(),
            dma((2, n_z - 1)), dma((2, n_z - 1, n_st)), dma((2, n_mates, n_st)), dma((PIECES,)), dma((PIECES,)),
        ]
        return pl.pallas_call(
            functools.partial(kernel, n_st, n_tp, cap, picks, held),
            out_shape=jax.ShapeDtypeStruct((total, heads * VALUE_DIM), BF16),
            in_specs=[smem] + [hbm] * 7 + [vmem] + [hbm] * 5,
            out_specs=vmem,
            scratch_shapes=scratch,
            compiler_params=pltpu.CompilerParams(
                collective_id=0, has_side_effects=True, vmem_limit_bytes=60 * 1024 * 1024),
        )(decay_rate, tokens, w_query, w_key, w_value, w_mem_query, w_mem_key, w_mem_value,
          w_gate.T, w_lift, jnp.asarray(cosine), jnp.asarray(sine), store, passage_ids.T)

    in_specs = (P("st", "tp"),) + (P(None, "tp"),) * 7 + (
        P("tp", None, None), P("tp"), P("st", None, "tp"), P("st", None))
    return jax.shard_map(per_device, mesh=mesh, in_specs=in_specs, out_specs=P("st", "tp"), check_vma=False)
```

time: 82.1 us -> 88.8 us (1.082); the launches traced: 80.9 us -> 88.5 us
  Pallas kernels: 79 us -> 86.7 us
    pallas_call x1, Pallas kernels: 79 us -> 86.7 us  [per_device(): pl.pallas_call(functools.partial(kernel, n_st, n_tp, cap, picks, held), o...]
where the time goes in v1:
time: 88.8 us; the launch traced here: 88.5 us
  Pallas kernels  86.7 us (98%)
  local copies, waits for them, and re-layouts  1.87 us (2%)
    pallas_call x1, Pallas kernels, per_device(): pl.pallas_call(functools.partial(kernel, n_st, n_tp, cap, picks, held), o...  86.7 us
    unnamed x1, local copies, waits for them, and re-layouts  1.87 us

profile of v1, /device:TPU:0, one launch (start us, length us, event | category | flops | bytes accessed | tf_op | source)
XLA Modules:
  0.0 88.5 jit_solution(1947373352850669825)
XLA Ops:
  0.0 86.7 %shard_map.136 = bf16[512,512]{1,0:T(8,128)(2,1)} custom-call(f32[2]{0:T(128)} %rate_ref.1, bf16[512,512]{1,0:T(8,128)(2,1)} %tok_hbm.1, bf16[4096,256]{1,0:T(8,128)(2,1)} %wq_hbm.1, bf16[4096,256]{1,0:T(8,128)(2,1)} %wk_hbm.1, bf16[4096,512]{1,0:T(8,128)(2,1)} %wv_hbm.1, bf16[4096,256]{1,0:T(8,128)(2,1)} %wm_hbm.1, bf16[4096,256]{1,0:T(8,128)(2,1)} %wmk_hbm.1, ...), custom_call_target="tpu_custom_call" | custom-call | tf_op jit(solution)/shard_map/pallas_call | solution.py:671
  86.7 1.9 %copy.16 = bf16[512,512]{1,0:T(8,128)(2,1)} copy(bf16[512,512]{1,0:T(8,128)(2,1)} %shard_map.136) | data formatting | bytes 1048576

commit v2 on v1

--- a/solution.py
+++ b/solution.py
@@ -79,6 +79,8 @@
     for i, (src, dst) in enumerate(pairs):
         loads.append(pltpu.make_async_copy(src, dst, load_sem.at[i]))
     loads[1].start()
+    loads[0].start()
+    loads[1].wait()
 
     barrier = pltpu.get_barrier_semaphore()
 
@@ -153,25 +155,8 @@
                         self.to_out(j, p).start()
                 self.to_pair(j, p).start()
 
-        def consume(self, side, d, first, last, take):
-            j, valid = self.at(side, d)
-
-            def step(q, carry):
-                p, which = first + q // CORES, q % CORES
-                this = j + which * (1 - 2 * core)
-
-                @pl.when(which == 1)
-                def _():
-                    self.to_pair(this, p).wait_recv()
-                take(this, p)
-                return carry
-
-            if d == 0:
-                lax.fori_loop(0, CORES * (last - first), step, 0)
-            else:
-                @pl.when(valid)
-                def _():
-                    lax.fori_loop(0, CORES * (last - first), step, 0)
+        def wait_pair(self, j, p):
+            self.to_pair(j + 1 - 2 * core, p).wait_recv()
 
         def drain(self):
             def step(p, carry):
@@ -208,117 +193,116 @@
     mates = row_mates + col_mates
     along_row = range(0, n_b - 1)
     along_col = range(n_b - 1, len(mates))
-    sub = CORES * cols // n_st
-    lent = 2 * (n_z - 1)
+    sub = CORES * cols // n_st // 2
+    others = n_z - 1
+    lent = 2 * others
+    late = lent - 2
     xw = (xwk, xwv)
 
-    def lent_at(e, s):
-        return pl.ds(pl.multiple_of((edge_z - so * (e + 1)) * (CORES * cols) + s * sub, sub), sub)
-
-    def lend(w):
-        kv, e = w % 2, w // 2
-        at = lent_at(e, st)
-        return remote((wmk_hbm, wmv_hbm)[kv].at[at], xw[kv].at[at], w_send.at[kv, e], w_recv.at[kv, e, st], st, me_in)
-
-    def spread(kv, e, s, i):
-        here = xw[kv].at[lent_at(e, s)]
-        return remote(here, here, spread_send.at[kv, i, s], w_recv.at[kv, e, s], mates[i], me)
-
-    def spread_own(w):
-        kv, e = w % 2, w // 2
-
+    def lent_at(e, half, s):
+        start = (edge_z - so * (e + 1)) * (CORES * cols) + (2 * s + half) * sub
+        return pl.ds(pl.multiple_of(start, sub), sub)
+
+    def lend(w, half):
+        kv, e = w // others, w % others
+        at = lent_at(e, half, st)
+        return remote((wmk_hbm, wmv_hbm)[kv].at[at], xw[kv].at[at], w_send.at[kv, e, half],
+                      w_recv.at[kv, e, half, st], st, me_in)
+
+    def lend_all(first, last):
+        for w in range(first, last):
+            for half in range(2):
+                lend(w, half).start()
+
+    def spread(w, half, s, i):
+        kv, e = w // others, w % others
+        here = xw[kv].at[lent_at(e, half, s)]
+        return remote(here, here, spread_send.at[kv, i, s], w_recv.at[kv, e, half, s], mates[i], me)
+
+    def spread_own(first, last):
         @pl.when(is_helper)
         def _():
-            spread(kv, e, st, 0).wait_recv()
-            for i in range(len(mates)):
-                spread(kv, e, st, i).start()
-
-    def spread_on(w):
-        kv, e = w % 2, w // 2
-
+            for w in range(first, last):
+                for half in range(2):
+                    spread(w, half, st, 0).wait_recv()
+                    for i in range(len(mates)):
+                        spread(w, half, st, i).start()
+
+    def spread_on(first, last):
         @pl.when(is_helper)
         def _():
-            for s in (row_mates, col_mates)[kv]:
-                spread(kv, e, s, 0).wait_recv()
-                for i in (along_col, along_row)[kv]:
-                    spread(kv, e, s, i).start()
-
-    def spread_last(w):
-        kv, e = w % 2, w // 2
+            for w in range(first, last):
+                for half in range(2):
+                    for s in (row_mates, col_mates)[half]:
+                        spread(w, half, s, 0).wait_recv()
+                        for i in (along_col, along_row)[half]:
+                            spread(w, half, s, i).start()
+
+    def spread_last(kv):
+        rest = ([(a + i) % n_a * n_b + k for i in range(1, n_a) for k in range(n_b)],
+                [k * n_b + (b + i) % n_b for i in range(1, n_b) for k in range(n_a)])
 
         @pl.when(is_helper)
         def _():
-            if kv == 0:
-                rest = [(a + i) % n_a * n_b + k for i in range(1, n_a) for k in range(n_b)]
-            else:
-                rest = [k * n_b + (b + i) % n_b for i in range(1, n_b) for k in range(n_a)]
-            for s in rest:
-                spread(kv, e, s, 0).wait_recv()
+            for w in range(kv * others, (kv + 1) * others):
+                for half in range(2):
+                    for s in rest[half]:
+                        spread(w, half, s, 0).wait_recv()
 
     def spread_drain():
-        def all_of(kv, s, i):
-            whole = xw[kv].at[pl.ds(0, (n_z - 1) * sub)]
-            return remote(whole, whole, spread_send.at[kv, i, s], w_recv.at[kv, 0, s], mates[i], me)
-
-        @pl.when(is_helper)
-        def _():
-            for kv in range(2):
-                for i in range(len(mates)):
-                    all_of(kv, st, i).wait_send()
-                for s in (row_mates, col_mates)[kv]:
-                    for i in (along_col, along_row)[kv]:
-                        all_of(kv, s, i).wait_send()
-
-        @pl.when(is_edge)
-        def _():
-            for w in range(lent):
-                lend(w).wait_send()
-
-    def kv_copy(p):
-        at = pl.ds(p * rows_piece, rows_piece)
-        return remote(kv_out.at[at], kv_in.at[at], kv_send.at[p], kv_recv.at[p], st, me_out)
+        def all_of(kv, s, i, halves):
+            whole = xw[kv].at[pl.ds(0, others * sub * halves)]
+            return remote(whole, whole, spread_send.at[kv, i, s], w_recv.at[kv, 0, 0, s], mates[i], me)
+
+        for kv in range(2):
+            for i in range(len(mates)):
+                all_of(kv, st, i, 2).wait_send()
+            for half in range(2):
+                for s in (row_mates, col_mates)[half]:
+                    for i in (along_col, along_row)[half]:
+                        all_of(kv, s, i, 1).wait_send()
+
+    def kv_copy(kv, p):
+        at = pl.ds(pl.multiple_of(p * rows_piece, rows_piece), rows_piece)
+        return remote(kv_out.at[kv, at], kv_in.at[kv, at], kv_send.at[kv, p], kv_recv.at[kv, p], st, me_out)
 
     def id_copy(d):
-        return remote(ids_hbm, ids_v.at[st], id_send.at[d], id_recv.at[st], (st + d) % n_st, me)
+        return remote(ids_v.at[st], ids_v.at[st], id_send.at[d], id_recv.at[st], (st + d) % n_st, me)
 
     def id_wait(d):
         other = (st + d) % n_st
-        return remote(ids_hbm, ids_v.at[other], id_send.at[d], id_recv.at[other], other, me)
+        return remote(ids_v.at[other], ids_v.at[other], id_send.at[d], id_recv.at[other], other, me)
 
     half = PIECES // 2
-    late = lent - 2
     for d in range(1, n_st):
         id_copy(d).start()
-    for p in range(half):
-        @pl.when(is_edge)
-        def _():
-            lend(p).start()
-        toks.send_own(p)
 
     @pl.when(is_edge)
     def _():
-        for w in range(half, late):
-            lend(w).start()
+        for p in range(half):
+            lend_all(p, p + 1)
+            toks.send_own(p)
+        lend_all(half, late)
 
     @pl.when(depth > 0)
     def _():
-        for p in range(half, PIECES):
+        for p in range(PIECES):
             toks.send_own(p)
-    loads[0].start()
     for p in range(PIECES):
         toks.share_own(p)
     loads[2].start()
 
-    for ref in (acc_q, acc_k, acc_v, acc_m, acc_g, acc_s, acc_mk, acc_mv):
+    for ref in (acc_q, acc_k, acc_v, acc_m, acc_g, acc_s):
         ref[...] = jnp.zeros_like(ref)
 
-    loads[1].wait()
     for d in range(1, n_st):
         id_wait(d).wait_recv()
     to_scalar = pltpu.make_async_copy(ids_v, ids_s, load_sem.at[len(pairs)])
     to_scalar.start()
     to_scalar.wait()
     loads[0].wait()
+    for i in range(3, len(pairs)):
+        loads[i].start()
 
     def asked(source, k):
         found = jnp.int32(0)
@@ -349,8 +333,6 @@
             pass_copy(g, d).start()
     for k in range(cap):
         landed[k // per][st, k % per] = store[asked(st, k)]
-    for i in range(3, len(pairs)):
-        loads[i].start()
 
     def build(block):
         reach = min(parts, -(-picks * (block + 1) // per))
@@ -370,31 +352,63 @@
         for block in range(p * blocks // PIECES, (p + 1) * blocks // PIECES):
             build(block)
 
-    def take_tokens(j, p):
-        at = pl.ds(pl.multiple_of(j * cols, cols), cols)
-        here = pl.ds(pl.multiple_of(p * chunk, chunk), chunk)
-        x = tok[j, here, :]
-        acc_q[here, :] += dot(x, wq[at, :])
-        acc_k[here, :] += dot(x, wk[at, :])
-        acc_v[here, :] += dot(x, wv[at, :])
-        acc_m[here, :] += dot(x, wm[at, :])
-        wide = x.astype(F32)
-        if heads > 1:
-            acc_g[here, :] += dot_nt(x, wg_ref[:, at])
+    def take_tokens(at_z, h):
+        here = pl.ds(pl.multiple_of(h * (half * chunk), half * chunk), half * chunk)
+        xs, ats = [], []
+        for c in range(CORES):
+            j = at_z * CORES + c
+            xs.append(tok[j, here, :])
+            ats.append(pl.ds(pl.multiple_of(j * cols, cols), cols))
+        for acc, w in ((acc_q, wq), (acc_k, wk), (acc_v, wv), (acc_m, wm)):
+            acc[here, :] += sum(dot(x, w[at, :]) for x, at in zip(xs, ats))
+        squares = acc_s[here, :]
+        for x, at in zip(xs, ats):
+            wide = x.astype(F32)
+            if heads > 1:
+                acc_g[here, :] += dot_nt(x, wg_ref[:, at])
+            else:
+                acc_g[here, :] += jnp.sum(wide * wg_ref[:, at].astype(F32), axis=1, keepdims=True)
+            for piece in range(cols // 128):
+                slab = wide[:, piece * 128:(piece + 1) * 128]
+                squares = squares + slab * slab
+        acc_s[here, :] = squares
+
+    def tokens_of(side, d, h):
+        j, valid = toks.at(side, d)
+
+        def go():
+            for p in range(half):
+                toks.wait_pair(j, h * half + p)
+            take_tokens(j // CORES, h)
+        if d == 0:
+            go()
         else:
-            acc_g[here, :] += jnp.sum(wide * wg_ref[:, at].astype(F32), axis=1, keepdims=True)
-        squares = acc_s[here, :]
-        for piece in range(cols // 128):
-            slab = wide[:, piece * 128:(piece + 1) * 128]
-            squares = squares + slab * slab
-        acc_s[here, :] = squares
-
-    def take_rows(j, p):
-        at = pl.ds(pl.multiple_of(j * cols, cols), cols)
-        here = pl.ds(pl.multiple_of(p * rows_piece, rows_piece), rows_piece)
-        x = rows[j, here, :]
-        acc_mk[here, :] += dot(x, wmk[at, :])
-        acc_mv[here, :] += dot(x, wmv[at, :])
+            pl.when(valid)(go)
+
+    def rows_wait(p):
+        for side, distances in ((IN, [0]), (OUT, outs), (IN, ins)):
+            for d in distances:
+                j, valid = passes.at(side, d)
+                if d == 0:
+                    passes.wait_pair(j, p)
+                else:
+                    @pl.when(valid)
+                    def _():
+                        passes.wait_pair(j, p)
+
+    def project(p, base, count, w):
+        at = pl.ds(p * rows_piece, rows_piece)
+        total_of = None
+        for q in range(count):
+            j = base + q
+            part = dot(rows[j, at, :], w[pl.ds(pl.multiple_of(j * cols, cols), cols), :])
+            total_of = part if total_of is None else total_of + part
+        return total_of
+
+    def rows_all(p, base, count):
+        at = pl.ds(p * rows_piece, rows_piece)
+        acc_mk[at, :] = project(p, base, count, wmk)
+        acc_mv[at, :] = project(p, base, count, wmv)
 
     def prepare(c, carry):
         here = pl.ds(pl.multiple_of(c * chunk, chunk), chunk)
@@ -433,19 +447,13 @@
             o = o - jnp.mean(o, axis=1, keepdims=True)
             ret[here, wide] = o * lax.rsqrt(jnp.mean(o * o, axis=1, keepdims=True) + NORM_EPS)
 
-    def assist(p):
+    def assist(kv, p):
         @pl.when(is_helper)
         def _():
-            at = pl.ds(pl.multiple_of(p * rows_piece, rows_piece), rows_piece)
+            at = pl.ds(p * rows_piece, rows_piece)
             base = jnp.where(so < 0, CORES, 0)
-            for kv in range(2):
-                total_kv = None
-                for q in range(CORES * (n_z - 1)):
-                    j = base + q
-                    part = dot(rows[j, at, :], xw[kv][pl.ds(pl.multiple_of(j * cols, cols), cols), :])
-                    total_kv = part if total_kv is None else total_kv + part
-                kv_out[at, kv * mem_cols:(kv + 1) * mem_cols] = total_kv.astype(BF16)
-            kv_copy(p).start()
+            kv_out[kv, at, :] = project(p, base, CORES * others, xw[kv]).astype(BF16)
+            kv_copy(kv, p).start()
 
     block = total // blocks
     keys = picks * pass_rows
@@ -466,138 +474,188 @@
             out_ref[here, wide] = (ret[here, wide] + gate[here, h:h + 1] * lifted).astype(BF16)
         return carry
 
-    def tokens_of(side, d, first, last):
-        toks.consume(side, d, first, last, take_tokens)
-
-    def rows_of(side, d, p):
-        passes.consume(side, d, p, p + 1, take_rows)
-
-    for p in range(half):
-        toks.relay(IN, 1, p)
-        spread_own(p)
+    share = blocks // PIECES
+
+    def attend_piece(p):
+        for n in range(p * share, (p + 1) * share):
+            attend(n, 0)
+
+    def pass_waits(first, last):
+        for g in range(first, last):
+            for d in range(1, n_st):
+                pass_wait(g, d).wait_recv()
+
+    def load_waits():
+        for i in range(2, len(pairs)):
+            loads[i].wait()
+
+    def settle(c):
+        prepare(c, 0)
+        retain(c)
+
+    early_parts = min(parts, -(-picks * share // per))
+
+    def in_tokens(p, distances):
+        for d in distances:
+            toks.relay(IN, d, p)
+
+    def out_tokens(p):
         for d in outs:
             toks.relay(OUT, d, p)
-    for i in range(2, len(pairs)):
-        loads[i].wait()
-    tokens_of(IN, 0, 0, PIECES)
-    for p in range(half, PIECES):
-        toks.relay(IN, 1, p)
-
-    for d in range(1, n_st):
-        pass_wait(0, d).wait_recv()
-    first_needs = min(parts, -(-picks * (blocks // PIECES) // per))
-    for g in range(1, first_needs):
-        for d in range(1, n_st):
-            pass_wait(g, d).wait_recv()
-    build_piece(0)
-    passes.send_own(0)
-    passes.share_own(0)
+
+    def in_rows(p, distances):
+        for d in distances:
+            passes.relay(IN, d, p)
+
+    def out_rows(p):
+        for d in outs:
+            passes.relay(OUT, d, p)
+
+    near, far = ins[:1], ins[1:]
 
     @pl.when(is_edge)
     def _():
+        in_tokens(0, near)
+        in_tokens(1, near)
+        pass_waits(0, early_parts)
+        build_piece(0)
+        passes.send_own(0)
+        passes.share_own(0)
         for p in range(half, PIECES):
             toks.send_own(p)
-        for w in range(late, lent):
-            lend(w).start()
-
-    tokens_of(IN, 1, 0, PIECES)
-    for w in range(half, late):
-        spread_own(w)
-    for p in range(half):
-        toks.relay(IN, 2, p)
-    for d in outs:
-        tokens_of(OUT, d, 0, half)
-    tokens_of(IN, 2, 0, half)
-
-    for g in range(first_needs, parts):
-        for d in range(1, n_st):
-            pass_wait(g, d).wait_recv()
-    for p in range(1, PIECES):
-        build_piece(p)
-        passes.share_own(p)
-    passes.send_own(1)
-
-    @pl.when(is_edge)
-    def _():
-        for p in range(2, PIECES):
+        lend_all(late, lent)
+        in_tokens(2, near)
+        load_waits()
+        tokens_of(IN, 0, 0)
+        in_tokens(3, near)
+        pass_waits(early_parts, parts)
+        for p in range(1, PIECES):
+            build_piece(p)
             passes.send_own(p)
-
-    for d in outs:
-        passes.relay(OUT, d, 0)
-    passes.relay(IN, 1, 0)
-    for w in range(half):
-        spread_on(w)
-    for p in range(half, PIECES):
-        for d in outs:
-            toks.relay(OUT, d, p)
+            passes.share_own(p)
+        tokens_of(IN, 0, 1)
+        in_tokens(0, ins[1:2])
+        tokens_of(IN, 1, 0)
+        in_tokens(1, ins[1:2])
+        tokens_of(IN, 1, 1)
+        in_tokens(2, ins[1:2])
+        tokens_of(IN, 2, 0)
+        in_tokens(3, ins[1:2])
+        tokens_of(IN, 2, 1)
+        for p in range(PIECES):
+            passes.wait_pair(me, p)
+            rows_all(p, z * CORES, CORES)
+        for d in ins[2:]:
+            in_tokens(0, [d])
+            in_tokens(1, [d])
+            tokens_of(IN, d, 0)
+        settle(0)
+        settle(1)
+        for d in ins[2:]:
+            in_tokens(2, [d])
+            in_tokens(3, [d])
+            tokens_of(IN, d, 1)
+        settle(2)
+        settle(3)
+        for p in range(PIECES):
+            at = pl.ds(p * rows_piece, rows_piece)
+            for kv, acc in ((0, acc_mk), (1, acc_mv)):
+                kv_copy(kv, p).wait_recv()
+                acc[at, :] += kv_in[kv, at, :].astype(F32)
+            attend_piece(p)
+        for w in range(lent):
+            for part in range(2):
+                lend(w, part).wait_send()
 
     @pl.when(depth > 0)
     def _():
-        for p in range(2, PIECES):
+        in_tokens(0, near)
+        spread_own(0, 1)
+        in_tokens(1, near)
+        out_tokens(0)
+        in_tokens(2, near)
+        spread_own(1, 2)
+        pass_waits(0, early_parts)
+        build_piece(0)
+        passes.send_own(0)
+        passes.share_own(0)
+        in_tokens(3, near)
+        out_tokens(1)
+        load_waits()
+        tokens_of(IN, 0, 0)
+        in_tokens(0, far)
+        spread_own(2, 3)
+        pass_waits(early_parts, parts)
+        for p in range(1, PIECES):
+            build_piece(p)
             passes.send_own(p)
-
-    for d in ins[1:]:
-        passes.relay(IN, d, 0)
-    for p in range(half, PIECES):
-        toks.relay(IN, 2, p)
-    for d in ins[2:]:
-        for p in range(half):
-            toks.relay(IN, d, p)
-        tokens_of(IN, d, 0, half)
-    for c in range(half):
-        prepare(c, 0)
-        retain(c)
-    for w in range(half, late):
-        spread_on(w)
-    for w in range(late, lent):
-        spread_own(w)
-    for d in outs:
-        tokens_of(OUT, d, half, PIECES)
-    tokens_of(IN, 2, half, PIECES)
-    for d in ins[2:]:
-        for p in range(half, PIECES):
-            toks.relay(IN, d, p)
-        tokens_of(IN, d, half, PIECES)
-
-    def rows_relay(p):
+            passes.share_own(p)
+        tokens_of(IN, 0, 1)
+        in_rows(0, near)
+        spread_own(3, late)
+        tokens_of(IN, 1, 0)
+        in_tokens(1, far)
+        out_rows(0)
+        tokens_of(IN, 1, 1)
         for d in outs:
-            passes.relay(OUT, d, p)
-        for d in ins:
-            passes.relay(IN, d, p)
-
-    def rows_take(p):
-        rows_of(IN, 0, p)
+            tokens_of(OUT, d, 0)
+        out_tokens(2)
+        in_rows(1, near)
+        spread_on(0, others - 1)
+        for d in far:
+            tokens_of(IN, d, 0)
+        out_tokens(3)
+        in_rows(2, near)
+        spread_on(others - 1, others)
+        settle(0)
+        settle(1)
+        in_rows(3, near)
+        spread_own(late, late + 1)
+        in_rows(0, far)
+        rows_wait(0)
+        spread_own(late + 1, lent)
+        spread_last(0)
+        assist(0, 0)
+        spread_on(others, late)
         for d in outs:
-            rows_of(OUT, d, p)
-        for d in ins:
-            rows_of(IN, d, p)
-
-    rows_relay(1)
-    for w in range(late, lent):
-        spread_on(w)
-    for c in range(half, PIECES):
-        prepare(c, 0)
-        retain(c)
-    for w in range(lent):
-        spread_last(w)
-
-    def finish(p, carry):
-        @pl.when(p > 1)
+            tokens_of(OUT, d, 1)
+        in_tokens(2, far)
+        out_rows(1)
+        spread_on(late, late + 1)
+        in_tokens(3, far)
+        out_rows(2)
+        spread_on(late + 1, lent)
+        for d in far:
+            tokens_of(IN, d, 1)
+        out_rows(3)
+        in_rows(1, far)
+        rows_wait(1)
+        assist(0, 1)
+        spread_last(1)
+        assist(1, 0)
+        assist(1, 1)
+        settle(2)
+        settle(3)
+        in_rows(2, far)
+        rows_wait(2)
+        assist(0, 2)
+        assist(1, 2)
+        rows_all(0, 0, n_tp)
+        attend_piece(0)
+        in_rows(3, far)
+        rows_wait(3)
+        assist(0, 3)
+        assist(1, 3)
+        for p in range(1, PIECES):
+            rows_all(p, 0, n_tp)
+            attend_piece(p)
+
+        @pl.when(is_helper)
         def _():
-            rows_relay(p)
-        rows_take(p)
-        assist(p)
-
-        @pl.when(is_edge)
-        def _():
-            at = pl.ds(pl.multiple_of(p * rows_piece, rows_piece), rows_piece)
-            kv_copy(p).wait_recv()
-            acc_mk[at, :] += kv_in[at, :mem_cols].astype(F32)
-            acc_mv[at, :] += kv_in[at, mem_cols:].astype(F32)
-        share = blocks // PIECES
-        lax.fori_loop(p * share, (p + 1) * share, attend, 0)
-        return carry
-    lax.fori_loop(0, PIECES, finish, 0)
+            spread_drain()
+            for kv in range(2):
+                for p in range(PIECES):
+                    kv_copy(kv, p).wait_send()
 
     for d in range(1, n_st):
         id_copy(d).wait_send()
@@ -605,12 +663,6 @@
             pass_copy(g, d).wait_send()
     toks.drain()
     passes.drain()
-    spread_drain()
-
-    @pl.when(is_helper)
-    def _():
-        for p in range(PIECES):
-            kv_copy(p).wait_send()
 
 
 def rotary_tables(total):
@@ -663,10 +715,10 @@
             V((total, key_cols), BF16), V((total, key_cols), BF16), V((total, wide), BF16), V((total, mem_cols), BF16),
             V((total, wide), F32), V((total, heads), F32),
             V(w_mem_key.shape, BF16), V(w_mem_value.shape, BF16),
-            V((all_rows, 2 * mem_cols), BF16), V((all_rows, 2 * mem_cols), BF16),
+            V((2, all_rows, mem_cols), BF16), V((2, all_rows, mem_cols), BF16),
             dma((16,)), dma((n_st,)), dma((n_st,)), dma((parts, n_st)), dma((parts, n_st)),
             flow_sems(), flow_sems(),
-            dma((2, n_z - 1)), dma((2, n_z - 1, n_st)), dma((2, n_mates, n_st)), dma((PIECES,)), dma((PIECES,)),
+            dma((2, n_z - 1, 2)), dma((2, n_z - 1, 2, n_st)), dma((2, n_mates, n_st)), dma((2, PIECES)), dma((2, PIECES)),
         ]
         return pl.pallas_call(
             functools.partial(kernel, n_st, n_tp, cap, picks, held),

time: 88.8 us -> 69.1 us (0.78)
  Pallas kernels: 86.7 us -> 67 us
    pallas_call x1, Pallas kernels: 86.7 us -> 67 us  [per_device(): pl.pallas_call(functools.partial(kernel, n_st, n_tp, cap, picks, held), o...]
where the time goes in v2:
time: 69.1 us; the launch traced here: 68.9 us
  Pallas kernels  67 us (97%)
  local copies, waits for them, and re-layouts  1.87 us (3%)
    pallas_call x1, Pallas kernels, per_device(): pl.pallas_call(functools.partial(kernel, n_st, n_tp, cap, picks, held), o...  67 us
    unnamed x1, local copies, waits for them, and re-layouts  1.87 us

profile of v2, /device:TPU:0, one launch (start us, length us, event | category | flops | bytes accessed | tf_op | source)
XLA Modules:
  0.0 68.9 jit_solution(16560881509902720627)
XLA Ops:
  0.0 67.0 %shard_map.136 = bf16[512,512]{1,0:T(8,128)(2,1)} custom-call(f32[2]{0:T(128)} %rate_ref.1, bf16[512,512]{1,0:T(8,128)(2,1)} %tok_hbm.1, bf16[4096,256]{1,0:T(8,128)(2,1)} %wq_hbm.1, bf16[4096,256]{1,0:T(8,128)(2,1)} %wk_hbm.1, bf16[4096,512]{1,0:T(8,128)(2,1)} %wv_hbm.1, bf16[4096,256]{1,0:T(8,128)(2,1)} %wm_hbm.1, bf16[4096,256]{1,0:T(8,128)(2,1)} %wmk_hbm.1, ...), custom_call_target="tpu_custom_call" | custom-call | tf_op jit(solution)/shard_map/pallas_call | solution.py:723
  67.0 1.9 %copy.16 = bf16[512,512]{1,0:T(8,128)(2,1)} copy(bf16[512,512]{1,0:T(8,128)(2,1)} %shard_map.136) | data formatting | bytes 1048576

commit v3 on v2

--- a/solution.py
+++ b/solution.py
@@ -43,7 +43,7 @@
     acc_q, acc_k, acc_v, acc_m, acc_g, acc_s, acc_mk, acc_mv,
     rq, rk, rv, mq, ret, gate, xwk, xwv, kv_out, kv_in,
     load_sem, id_send, id_recv, pass_send, pass_recv,
-    t_sems, r_sems, w_send, w_recv, spread_send, kv_send, kv_recv,
+    t_sems, r_sems, w_send, w_own, w_row, w_col, w_final, spread_send, kv_send, kv_recv,
 ):
     st = lax.axis_index("st")
     me = lax.axis_index("tp")
@@ -60,6 +60,7 @@
     per = cap // parts
     chunk = total // PIECES
     rows_piece = rows.shape[1] // PIECES
+    half = PIECES // 2
 
     so = jnp.where(z < n_z // 2, -1, 1)
     depth = jnp.minimum(z, n_z - 1 - z)
@@ -80,7 +81,6 @@
         loads.append(pltpu.make_async_copy(src, dst, load_sem.at[i]))
     loads[1].start()
     loads[0].start()
-    loads[1].wait()
 
     barrier = pltpu.get_barrier_semaphore()
 
@@ -102,9 +102,9 @@
             device_id=(to_st, to_tp), device_id_type=MESH)
 
     class Flow:
-        def __init__(self, buf, sems, floor, source=None):
-            self.buf, self.floor, self.source = buf, floor, source
-            self.recv, self.send, self.own_out, self.pairing = sems
+        def __init__(self, buf, sems, floor, pair_sem, source=None):
+            self.buf, self.floor, self.source, self.pair_sem = buf, floor, source, pair_sem
+            self.recv, self.recv_pair, self.send, self.own_out, self.send_pair = sems
             self.size = buf.shape[1] // PIECES
 
         def piece(self, j, p):
@@ -113,24 +113,20 @@
         def origin(self, p):
             return self.piece(me, p) if self.source is None else self.source.at[pl.ds(p * self.size, self.size)]
 
-        def copy(self, j, p, sem, to, src=None):
-            return remote(self.piece(j, p) if src is None else src, self.piece(j, p), sem, self.recv.at[j, p], st, to)
-
-        def to_in(self, j, p, src=None):
-            return self.copy(j, p, self.send.at[j, p], me_in, src)
-
-        def to_out(self, j, p, src=None):
-            return self.copy(j, p, self.send.at[j, p] if src is None else self.own_out.at[p], me_out, src)
+        def along_z(self, j, p, to, src=None, send=None):
+            return remote(self.piece(j, p) if src is None else src, self.piece(j, p),
+                          self.send.at[j // CORES] if send is None else send, self.recv.at[j // CORES, p], st, to)
 
         def to_pair(self, j, p, src=None):
-            return self.copy(j, p, self.pairing.at[j, p], pair, src)
+            return remote(self.piece(j, p) if src is None else src, self.piece(j, p),
+                          self.send_pair.at[0], self.pair_sem(self.recv_pair, j // CORES, p), st, pair)
 
         def send_own(self, p):
-            self.to_in(me, p, self.origin(p)).start()
+            self.along_z(me, p, me_in, self.origin(p)).start()
 
             @pl.when(depth > self.floor)
             def _():
-                self.to_out(me, p, self.origin(p)).start()
+                self.along_z(me, p, me_out, self.origin(p), self.own_out.at[0]).start()
 
         def share_own(self, p):
             self.to_pair(me, p, self.origin(p)).start()
@@ -146,44 +142,44 @@
 
             @pl.when(valid)
             def _():
-                self.to_pair(j, p).wait_recv()
+                self.along_z(j, p, me_in).wait_recv()
                 if side == OUT:
-                    self.to_in(j, p).start()
+                    self.along_z(j, p, me_in).start()
                 else:
                     @pl.when(depth > self.floor)
                     def _():
-                        self.to_out(j, p).start()
+                        self.along_z(j, p, me_out).start()
                 self.to_pair(j, p).start()
 
-        def wait_pair(self, j, p):
-            self.to_pair(j + 1 - 2 * core, p).wait_recv()
+        def wait_pair(self, ref, sem):
+            remote(ref, ref, self.send_pair.at[0], sem, st, pair).wait_recv()
 
         def drain(self):
-            def step(p, carry):
-                self.to_in(me, p, self.origin(p)).wait_send()
-                self.to_pair(me, p, self.origin(p)).wait_send()
-
-                @pl.when(depth > self.floor)
-                def _():
-                    self.to_out(me, p, self.origin(p)).wait_send()
-                for side, distances in ((OUT, outs), (IN, ins)):
-                    for d in distances:
-                        j, valid = self.at(side, d)
-
-                        @pl.when(valid)
-                        def _():
-                            if side == OUT:
-                                self.to_in(j, p).wait_send()
-                            else:
-                                @pl.when(depth > self.floor)
-                                def _():
-                                    self.to_out(j, p).wait_send()
-                            self.to_pair(j, p).wait_send()
-                return carry
-            lax.fori_loop(0, PIECES, step, 0)
-
-    toks = Flow(tok, t_sems, 0, tok_hbm)
-    passes = Flow(rows, r_sems, 1)
+            def sent(ref, sem):
+                remote(ref, ref, sem, self.recv.at[0, 0], st, me_in).wait_send()
+            sent(self.buf.at[0], self.send.at[z])
+
+            @pl.when(depth > self.floor)
+            def _():
+                sent(self.buf.at[0], self.own_out.at[0])
+            for side, distances in ((OUT, outs), (IN, ins)):
+                for d in distances:
+                    j, valid = self.at(side, d)
+
+                    @pl.when(valid if side == OUT else valid & (depth > self.floor))
+                    def _():
+                        sent(self.buf.at[0], self.send.at[j // CORES])
+
+            @pl.when(depth >= self.floor)
+            def _():
+                sent(self.buf.at[pl.ds(0, n_z)], self.send_pair.at[0])
+
+            @pl.when(depth < self.floor)
+            def _():
+                sent(self.buf.at[0], self.send_pair.at[0])
+
+    toks = Flow(tok, t_sems, 0, lambda sems, chip, p: sems.at[chip, p // half], tok_hbm)
+    passes = Flow(rows, r_sems, 1, lambda sems, chip, p: sems.at[p])
 
     n_b = square_split(n_st)
     n_a = n_st // n_b
@@ -199,72 +195,72 @@
     late = lent - 2
     xw = (xwk, xwv)
 
-    def lent_at(e, half, s):
-        start = (edge_z - so * (e + 1)) * (CORES * cols) + (2 * s + half) * sub
-        return pl.ds(pl.multiple_of(start, sub), sub)
-
-    def lend(w, half):
+    def lent_at(e, part, s, count=1):
+        start = (edge_z - so * (e + 1)) * (CORES * cols) + (2 * s + part) * sub
+        return pl.ds(pl.multiple_of(start, sub), sub * count)
+
+    def lend(w):
         kv, e = w // others, w % others
-        at = lent_at(e, half, st)
-        return remote((wmk_hbm, wmv_hbm)[kv].at[at], xw[kv].at[at], w_send.at[kv, e, half],
-                      w_recv.at[kv, e, half, st], st, me_in)
+        at = lent_at(e, 0, st, 2)
+        return remote((wmk_hbm, wmv_hbm)[kv].at[at], xw[kv].at[at], w_send.at[0], w_own.at[w], st, me_in)
 
     def lend_all(first, last):
         for w in range(first, last):
-            for half in range(2):
-                lend(w, half).start()
-
-    def spread(w, half, s, i):
+            lend(w).start()
+
+    def spread(w, part, s, i, send, recv):
         kv, e = w // others, w % others
-        here = xw[kv].at[lent_at(e, half, s)]
-        return remote(here, here, spread_send.at[kv, i, s], w_recv.at[kv, e, half, s], mates[i], me)
+        here = xw[kv].at[lent_at(e, part, s)]
+        return remote(here, here, spread_send.at[send], recv, mates[i], me)
 
     def spread_own(first, last):
         @pl.when(is_helper)
         def _():
             for w in range(first, last):
-                for half in range(2):
-                    spread(w, half, st, 0).wait_recv()
-                    for i in range(len(mates)):
-                        spread(w, half, st, i).start()
+                lend(w).wait_recv()
+                for part in range(2):
+                    for i in along_row:
+                        recv = w_row.at[w, n_b - 2 - i] if part == 0 else w_final.at[w // others]
+                        spread(w, part, st, i, 0, recv).start()
+                    for i in along_col:
+                        recv = w_col.at[w, n_a - 2 - (i - (n_b - 1))] if part == 1 else w_final.at[w // others]
+                        spread(w, part, st, i, 0, recv).start()
 
     def spread_on(first, last):
         @pl.when(is_helper)
         def _():
             for w in range(first, last):
-                for half in range(2):
-                    for s in (row_mates, col_mates)[half]:
-                        spread(w, half, s, 0).wait_recv()
-                        for i in (along_col, along_row)[half]:
-                            spread(w, half, s, i).start()
+                final = w_final.at[w // others]
+                for k, s in enumerate(row_mates):
+                    spread(w, 0, s, 0, 1, w_row.at[w, k]).wait_recv()
+                    for i in along_col:
+                        spread(w, 0, s, i, 1, final).start()
+                for k, s in enumerate(col_mates):
+                    spread(w, 1, s, 0, 1, w_col.at[w, k]).wait_recv()
+                    for i in along_row:
+                        spread(w, 1, s, i, 1, final).start()
+
+    def lent_rows(count):
+        return xwk.at[pl.ds(0, count * sub)]
 
     def spread_last(kv):
-        rest = ([(a + i) % n_a * n_b + k for i in range(1, n_a) for k in range(n_b)],
-                [k * n_b + (b + i) % n_b for i in range(1, n_b) for k in range(n_a)])
-
         @pl.when(is_helper)
         def _():
-            for w in range(kv * others, (kv + 1) * others):
-                for half in range(2):
-                    for s in rest[half]:
-                        spread(w, half, s, 0).wait_recv()
+            whole = lent_rows(others * (n_b * (n_a - 1) + n_a * (n_b - 1)))
+            remote(whole, whole, spread_send.at[0], w_final.at[kv], st, me_in).wait_recv()
 
     def spread_drain():
-        def all_of(kv, s, i, halves):
-            whole = xw[kv].at[pl.ds(0, others * sub * halves)]
-            return remote(whole, whole, spread_send.at[kv, i, s], w_recv.at[kv, 0, 0, s], mates[i], me)
-
-        for kv in range(2):
-            for i in range(len(mates)):
-                all_of(kv, st, i, 2).wait_send()
-            for half in range(2):
-                for s in (row_mates, col_mates)[half]:
-                    for i in (along_col, along_row)[half]:
-                        all_of(kv, s, i, 1).wait_send()
+        for k, count in enumerate((2 * len(mates), 2 * (n_a - 1) * (n_b - 1))):
+            whole = lent_rows(2 * others * count)
+            remote(whole, whole, spread_send.at[k], w_final.at[0], st, me_in).wait_send()
+
+    def lend_drain():
+        whole = lent_rows(2 * others * 2)
+        remote(whole, whole, w_send.at[0], w_own.at[0], st, me_in).wait_send()
 
     def kv_copy(kv, p):
         at = pl.ds(pl.multiple_of(p * rows_piece, rows_piece), rows_piece)
-        return remote(kv_out.at[kv, at], kv_in.at[kv, at], kv_send.at[kv, p], kv_recv.at[kv, p], st, me_out)
+        return remote(kv_out.at[kv, at], kv_in.at[kv, at], kv_send.at[0], kv_recv.at[kv, p], st, me_out)
 
     def id_copy(d):
         return remote(ids_v.at[st], ids_v.at[st], id_send.at[d], id_recv.at[st], (st + d) % n_st, me)
@@ -273,7 +269,7 @@
         other = (st + d) % n_st
         return remote(ids_v.at[other], ids_v.at[other], id_send.at[d], id_recv.at[other], other, me)
 
-    half = PIECES // 2
+    loads[1].wait()
     for d in range(1, n_st):
         id_copy(d).start()
 
@@ -315,13 +311,13 @@
         return found
 
     def pass_copy(g, d):
-        return remote(slots.at[d, pl.ds(g * per, per)], landed[g].at[st], pass_send.at[g, d], pass_recv.at[g, st],
+        return remote(slots.at[d, pl.ds(g * per, per)], landed[g].at[st], pass_send.at[0], pass_recv.at[g],
                       (st + d) % n_st, me)
 
-    def pass_wait(g, d):
-        other = (st + d) % n_st
-        return remote(slots.at[d, pl.ds(g * per, per)], landed[g].at[other], pass_send.at[g, d],
-                      pass_recv.at[g, other], other, me)
+    def pass_waits(first, last):
+        for g in range(first, last):
+            all_of = landed[g].at[pl.ds(0, n_st - 1)]
+            remote(all_of, all_of, pass_send.at[0], pass_recv.at[g], (st + 1) % n_st, me).wait_recv()
 
     for g in range(parts):
         def fill(d, carry):
@@ -377,24 +373,16 @@
         j, valid = toks.at(side, d)
 
         def go():
-            for p in range(half):
-                toks.wait_pair(j, h * half + p)
+            toks.wait_pair(tok.at[j + 1 - 2 * core, pl.ds(h * half * chunk, half * chunk)],
+                           toks.recv_pair.at[j // CORES, h])
             take_tokens(j // CORES, h)
         if d == 0:
             go()
         else:
             pl.when(valid)(go)
 
-    def rows_wait(p):
-        for side, distances in ((IN, [0]), (OUT, outs), (IN, ins)):
-            for d in distances:
-                j, valid = passes.at(side, d)
-                if d == 0:
-                    passes.wait_pair(j, p)
-                else:
-                    @pl.when(valid)
-                    def _():
-                        passes.wait_pair(j, p)
+    def rows_wait(p, chips):
+        passes.wait_pair(rows.at[pl.ds(0, chips), pl.ds(p * rows_piece, rows_piece)], passes.recv_pair.at[p])
 
     def project(p, base, count, w):
         at = pl.ds(p * rows_piece, rows_piece)
@@ -479,11 +467,6 @@
     def attend_piece(p):
         for n in range(p * share, (p + 1) * share):
             attend(n, 0)
-
-    def pass_waits(first, last):
-        for g in range(first, last):
-            for d in range(1, n_st):
-                pass_wait(g, d).wait_recv()
 
     def load_waits():
         for i in range(2, len(pairs)):
@@ -543,7 +526,7 @@
         in_tokens(3, ins[1:2])
         tokens_of(IN, 2, 1)
         for p in range(PIECES):
-            passes.wait_pair(me, p)
+            rows_wait(p, 1)
             rows_all(p, z * CORES, CORES)
         for d in ins[2:]:
             in_tokens(0, [d])
@@ -563,9 +546,7 @@
                 kv_copy(kv, p).wait_recv()
                 acc[at, :] += kv_in[kv, at, :].astype(F32)
             attend_piece(p)
-        for w in range(lent):
-            for part in range(2):
-                lend(w, part).wait_send()
+        lend_drain()
 
     @pl.when(depth > 0)
     def _():
@@ -588,7 +569,8 @@
         pass_waits(early_parts, parts)
         for p in range(1, PIECES):
             build_piece(p)
-            passes.send_own(p)
+            if p < PIECES - 1:
+                passes.send_own(p)
             passes.share_own(p)
         tokens_of(IN, 0, 1)
         in_rows(0, near)
@@ -605,47 +587,48 @@
         for d in far:
             tokens_of(IN, d, 0)
         out_tokens(3)
+        passes.send_own(PIECES - 1)
         in_rows(2, near)
         spread_on(others - 1, others)
+        in_tokens(2, far)
+        spread_own(late, late + 1)
         settle(0)
         settle(1)
-        in_rows(3, near)
-        spread_own(late, late + 1)
-        in_rows(0, far)
-        rows_wait(0)
+        in_tokens(3, far)
         spread_own(late + 1, lent)
-        spread_last(0)
-        assist(0, 0)
         spread_on(others, late)
         for d in outs:
             tokens_of(OUT, d, 1)
-        in_tokens(2, far)
+        in_rows(3, near)
+        in_rows(0, far)
+        rows_wait(0, n_z)
+        spread_last(0)
+        assist(0, 0)
         out_rows(1)
         spread_on(late, late + 1)
-        in_tokens(3, far)
+        for d in far:
+            tokens_of(IN, d, 1)
         out_rows(2)
         spread_on(late + 1, lent)
-        for d in far:
-            tokens_of(IN, d, 1)
         out_rows(3)
         in_rows(1, far)
-        rows_wait(1)
+        rows_wait(1, n_z)
         assist(0, 1)
         spread_last(1)
         assist(1, 0)
         assist(1, 1)
+        in_rows(2, far)
         settle(2)
-        settle(3)
-        in_rows(2, far)
-        rows_wait(2)
+        rows_wait(2, n_z)
         assist(0, 2)
         assist(1, 2)
+        settle(3)
+        in_rows(3, far)
         rows_all(0, 0, n_tp)
-        attend_piece(0)
-        in_rows(3, far)
-        rows_wait(3)
+        rows_wait(3, n_z)
         assist(0, 3)
         assist(1, 3)
+        attend_piece(0)
         for p in range(1, PIECES):
             rows_all(p, 0, n_tp)
             attend_piece(p)
@@ -653,14 +636,12 @@
         @pl.when(is_helper)
         def _():
             spread_drain()
-            for kv in range(2):
-                for p in range(PIECES):
-                    kv_copy(kv, p).wait_send()
+            remote(kv_out, kv_in, kv_send.at[0], kv_recv.at[0, 0], st, me_out).wait_send()
 
     for d in range(1, n_st):
         id_copy(d).wait_send()
-        for g in range(parts):
-            pass_copy(g, d).wait_send()
+    all_slots = slots.at[pl.ds(1, n_st - 1)]
+    remote(all_slots, all_slots, pass_send.at[0], pass_recv.at[0], (st + 1) % n_st, me).wait_send()
     toks.drain()
     passes.drain()
 
@@ -696,10 +677,9 @@
         wide = w_value.shape[1]
         key_cols, mem_cols = w_query.shape[1], w_mem_query.shape[1]
         n_b = square_split(n_st)
-        n_mates = n_b - 1 + n_st // n_b - 1
-
-        def flow_sems():
-            return dma((n_tp, PIECES)), dma((n_tp, PIECES)), dma((PIECES,)), dma((n_tp, PIECES))
+
+        def flow_sems(*pair_shape):
+            return dma((n_z, PIECES)), dma(pair_shape), dma((n_z,)), dma((1,)), dma((1,))
         all_rows = requests * pass_rows
         scratch = [
             V((n_tp, total, cols), BF16), V((n_tp, all_rows, cols), BF16),
@@ -716,13 +696,14 @@
             V((total, wide), F32), V((total, heads), F32),
             V(w_mem_key.shape, BF16), V(w_mem_value.shape, BF16),
             V((2, all_rows, mem_cols), BF16), V((2, all_rows, mem_cols), BF16),
-            dma((16,)), dma((n_st,)), dma((n_st,)), dma((parts, n_st)), dma((parts, n_st)),
-            flow_sems(), flow_sems(),
-            dma((2, n_z - 1, 2)), dma((2, n_z - 1, 2, n_st)), dma((2, n_mates, n_st)), dma((2, PIECES)), dma((2, PIECES)),
+            dma((13,)), dma((n_st,)), dma((n_st,)), dma((1,)), dma((parts,)),
+            flow_sems(n_z, 2), flow_sems(PIECES),
+            dma((1,)), dma((2 * (n_z - 1),)), dma((2 * (n_z - 1), n_b - 1)), dma((2 * (n_z - 1), n_st // n_b - 1)),
+            dma((2,)), dma((2,)), dma((1,)), dma((2, PIECES)),
         ]
         return pl.pallas_call(
             functools.partial(kernel, n_st, n_tp, cap, picks, held),
-            out_shape=jax.ShapeDtypeStruct((total, heads * VALUE_DIM), BF16),
+            out_shape=pltpu.VMEM((total, heads * VALUE_DIM), BF16),
             in_specs=[smem] + [hbm] * 7 + [vmem] + [hbm] * 5,
             out_specs=vmem,
             scratch_shapes=scratch,

time: 69.1 us -> 65.3 us (0.945)
  Pallas kernels: 67 us -> 64.3 us
  local copies, waits for them, and re-layouts: 1.87 us -> 0.8 us
    pallas_call x1, Pallas kernels: 67 us -> 64.3 us  [per_device(): pl.pallas_call(functools.partial(kernel, n_st, n_tp, cap, picks, held), o...]
    unnamed x1, local copies, waits for them, and re-layouts: 1.87 us -> 0.8 us
where the time goes in v3:
time: 65.3 us; the launch traced here: 65.1 us
  Pallas kernels  64.3 us (98%)
  local copies, waits for them, and re-layouts  0.8 us (1%)
    pallas_call x1, Pallas kernels, per_device(): pl.pallas_call(functools.partial(kernel, n_st, n_tp, cap, picks, held), o...  64.3 us

profile of v3, /device:TPU:0, one launch (start us, length us, event | category | flops | bytes accessed | tf_op | source)
XLA Modules:
  0.0 65.1 jit_solution(13514708918457807114)
XLA Ops:
  0.0 64.3 %shard_map.136 = bf16[512,512]{1,0:T(8,128)(2,1)S(1)} custom-call(f32[2]{0:T(128)} %rate_ref.1, bf16[512,512]{1,0:T(8,128)(2,1)} %tok_hbm.1, bf16[4096,256]{1,0:T(8,128)(2,1)} %wq_hbm.1, bf16[4096,256]{1,0:T(8,128)(2,1)} %wk_hbm.1, bf16[4096,512]{1,0:T(8,128)(2,1)} %wv_hbm.1, bf16[4096,256]{1,0:T(8,128)(2,1)} %wm_hbm.1, bf16[4096,256]{1,0:T(8,128)(2,1)} %wmk_hbm.1, ...), custom_call_target="tpu_custom_call" | custom-call | tf_op jit(solution)/shard_map/pallas_call | solution.py:704
  64.3 0.8 %copy.16 = bf16[512,512]{1,0:T(8,128)(2,1)} copy(bf16[512,512]{1,0:T(8,128)(2,1)S(1)} %shard_map.136) | data formatting | bytes 1048576

commit v4 on v3

--- a/solution.py
+++ b/solution.py
@@ -34,12 +34,17 @@
     return 1 << ((n.bit_length() - 1) // 2)
 
 
+def row_bounds(blocks, keys):
+    cuts = [keys * n for n in range(blocks + 1)]
+    return cuts[:-1] + [cuts[-1] - keys // 2, cuts[-1]]
+
+
 def kernel(
     n_st, n_tp, cap, picks, held,
     rate_ref, tok_hbm, wq_hbm, wk_hbm, wv_hbm, wm_hbm, wmk_hbm, wmv_hbm, wg_ref, lift_hbm,
     cos_hbm, sin_hbm, store_hbm, ids_hbm,
     out_ref,
-    tok, rows, cos_ref, sin_ref, lift_ref, wq, wk, wv, wm, wmk, wmv, store, slots, landed, ids_v, ids_s,
+    tok, rows, cos_ref, sin_ref, lift_ref, wq, wk, wv, wm, wmk, wmv, store, slots, landed, ids_s,
     acc_q, acc_k, acc_v, acc_m, acc_g, acc_s, acc_mk, acc_mv,
     rq, rk, rv, mq, ret, gate, xwk, xwv, kv_out, kv_in,
     load_sem, id_send, id_recv, pass_send, pass_recv,
@@ -59,7 +64,10 @@
     parts = len(landed)
     per = cap // parts
     chunk = total // PIECES
-    rows_piece = rows.shape[1] // PIECES
+    block = total // blocks
+    keys = picks * pass_rows
+    row_cuts = row_bounds(blocks, keys)
+    row_pieces = len(row_cuts) - 1
     half = PIECES // 2
 
     so = jnp.where(z < n_z // 2, -1, 1)
@@ -74,7 +82,7 @@
     ins = range(1, n_z)
 
     loads = []
-    pairs = [(store_hbm, store), (ids_hbm, ids_v.at[st]), (tok_hbm, tok.at[me]), (wq_hbm, wq), (wk_hbm, wk),
+    pairs = [(store_hbm, store), (ids_hbm, ids_s.at[st]), (tok_hbm, tok.at[me]), (wq_hbm, wq), (wk_hbm, wk),
              (wv_hbm, wv), (wm_hbm, wm), (wmk_hbm, wmk), (wmv_hbm, wmv),
              (cos_hbm, cos_ref), (sin_hbm, sin_ref), (lift_hbm, lift_ref)]
     for i, (src, dst) in enumerate(pairs):
@@ -102,16 +110,19 @@
             device_id=(to_st, to_tp), device_id_type=MESH)
 
     class Flow:
-        def __init__(self, buf, sems, floor, pair_sem, source=None):
+        def __init__(self, buf, cuts, sems, floor, pair_sem, source=None):
             self.buf, self.floor, self.source, self.pair_sem = buf, floor, source, pair_sem
             self.recv, self.recv_pair, self.send, self.own_out, self.send_pair = sems
-            self.size = buf.shape[1] // PIECES
+            self.cuts = cuts
 
         def piece(self, j, p):
-            return self.buf.at[j, pl.ds(p * self.size, self.size)]
+            return self.buf.at[j, self.rows(p)]
+
+        def rows(self, p):
+            return pl.ds(self.cuts[p], self.cuts[p + 1] - self.cuts[p])
 
         def origin(self, p):
-            return self.piece(me, p) if self.source is None else self.source.at[pl.ds(p * self.size, self.size)]
+            return self.piece(me, p) if self.source is None else self.source.at[self.rows(p)]
 
         def along_z(self, j, p, to, src=None, send=None):
             return remote(self.piece(j, p) if src is None else src, self.piece(j, p),
@@ -178,8 +189,8 @@
             def _():
                 sent(self.buf.at[0], self.send_pair.at[0])
 
-    toks = Flow(tok, t_sems, 0, lambda sems, chip, p: sems.at[chip, p // half], tok_hbm)
-    passes = Flow(rows, r_sems, 1, lambda sems, chip, p: sems.at[p])
+    toks = Flow(tok, [chunk * p for p in range(PIECES + 1)], t_sems, 0, lambda sems, chip, p: sems.at[chip, p // half], tok_hbm)
+    passes = Flow(rows, row_cuts, r_sems, 1, lambda sems, chip, p: sems.at[p])
 
     n_b = square_split(n_st)
     n_a = n_st // n_b
@@ -192,7 +203,6 @@
     sub = CORES * cols // n_st // 2
     others = n_z - 1
     lent = 2 * others
-    late = lent - 2
     xw = (xwk, xwv)
 
     def lent_at(e, part, s, count=1):
@@ -259,15 +269,15 @@
         remote(whole, whole, w_send.at[0], w_own.at[0], st, me_in).wait_send()
 
     def kv_copy(kv, p):
-        at = pl.ds(pl.multiple_of(p * rows_piece, rows_piece), rows_piece)
+        at = passes.rows(p)
         return remote(kv_out.at[kv, at], kv_in.at[kv, at], kv_send.at[0], kv_recv.at[kv, p], st, me_out)
 
     def id_copy(d):
-        return remote(ids_v.at[st], ids_v.at[st], id_send.at[d], id_recv.at[st], (st + d) % n_st, me)
+        return remote(ids_s.at[st], ids_s.at[st], id_send.at[d], id_recv.at[st], (st + d) % n_st, me)
 
     def id_wait(d):
         other = (st + d) % n_st
-        return remote(ids_v.at[other], ids_v.at[other], id_send.at[d], id_recv.at[other], other, me)
+        return remote(ids_s.at[other], ids_s.at[other], id_send.at[d], id_recv.at[other], other, me)
 
     loads[1].wait()
     for d in range(1, n_st):
@@ -278,7 +288,8 @@
         for p in range(half):
             lend_all(p, p + 1)
             toks.send_own(p)
-        lend_all(half, late)
+        lend_all(half, others)
+        toks.send_own(half)
 
     @pl.when(depth > 0)
     def _():
@@ -293,9 +304,6 @@
 
     for d in range(1, n_st):
         id_wait(d).wait_recv()
-    to_scalar = pltpu.make_async_copy(ids_v, ids_s, load_sem.at[len(pairs)])
-    to_scalar.start()
-    to_scalar.wait()
     loads[0].wait()
     for i in range(3, len(pairs)):
         loads[i].start()
@@ -343,10 +351,6 @@
                 other = landed[g][owner, jnp.clip(order - g * per, 0, per - 1)]
                 value = jnp.where(order >= g * per, other, value)
             rows[me, pl.ds(i * pass_rows, pass_rows), :] = value
-
-    def build_piece(p):
-        for block in range(p * blocks // PIECES, (p + 1) * blocks // PIECES):
-            build(block)
 
     def take_tokens(at_z, h):
         here = pl.ds(pl.multiple_of(h * (half * chunk), half * chunk), half * chunk)
@@ -382,10 +386,9 @@
             pl.when(valid)(go)
 
     def rows_wait(p, chips):
-        passes.wait_pair(rows.at[pl.ds(0, chips), pl.ds(p * rows_piece, rows_piece)], passes.recv_pair.at[p])
-
-    def project(p, base, count, w):
-        at = pl.ds(p * rows_piece, rows_piece)
+        passes.wait_pair(rows.at[pl.ds(0, chips), passes.rows(p)], passes.recv_pair.at[p])
+
+    def project(at, base, count, w):
         total_of = None
         for q in range(count):
             j = base + q
@@ -393,10 +396,10 @@
             total_of = part if total_of is None else total_of + part
         return total_of
 
-    def rows_all(p, base, count):
-        at = pl.ds(p * rows_piece, rows_piece)
-        acc_mk[at, :] = project(p, base, count, wmk)
-        acc_mv[at, :] = project(p, base, count, wmv)
+    def rows_all(n, base, count):
+        at = pl.ds(n * keys, keys)
+        acc_mk[at, :] = project(at, base, count, wmk)
+        acc_mv[at, :] = project(at, base, count, wmv)
 
     def prepare(c, carry):
         here = pl.ds(pl.multiple_of(c * chunk, chunk), chunk)
@@ -438,35 +441,43 @@
     def assist(kv, p):
         @pl.when(is_helper)
         def _():
-            at = pl.ds(p * rows_piece, rows_piece)
+            at = passes.rows(p)
             base = jnp.where(so < 0, CORES, 0)
-            kv_out[kv, at, :] = project(p, base, CORES * others, xw[kv]).astype(BF16)
+            kv_out[kv, at, :] = project(at, base, CORES * others, xw[kv]).astype(BF16)
             kv_copy(kv, p).start()
 
-    block = total // blocks
-    keys = picks * pass_rows
-
-    def attend(n, carry):
-        here = pl.ds(pl.multiple_of(n * block, block), block)
-        there = pl.ds(pl.multiple_of(n * keys, keys), keys)
+    def attend_keys(n):
+        here, there = pl.ds(n * block, block), pl.ds(n * keys, keys)
+        state = []
+        for h in range(heads):
+            at = slice(h * MEM_DIM, (h + 1) * MEM_DIM)
+            k = acc_mk[there, at]
+            k = (k * lax.rsqrt(jnp.mean(k * k, axis=1, keepdims=True) + NORM_EPS)).astype(BF16)
+            exponent = jnp.exp(dot_nt(mq[here, at], k) * MEM_DIM ** (-0.5))
+            state.append((exponent.astype(BF16), jnp.sum(exponent, axis=1, keepdims=True)))
+        return state
+
+    def attend_values(n, state):
+        here, there = pl.ds(n * block, block), pl.ds(n * keys, keys)
         for h in range(heads):
             at = slice(h * MEM_DIM, (h + 1) * MEM_DIM)
             wide = slice(h * VALUE_DIM, (h + 1) * VALUE_DIM)
-            k = acc_mk[there, at]
-            k = (k * lax.rsqrt(jnp.mean(k * k, axis=1, keepdims=True) + NORM_EPS)).astype(BF16)
+            exponent, mass = state[h]
             v = acc_mv[there, at].astype(BF16)
-            exponent = jnp.exp(dot_nt(mq[here, at], k) * MEM_DIM ** (-0.5))
-            mass = jnp.sum(exponent, axis=1, keepdims=True)
-            o = (dot(exponent.astype(BF16), v) / mass).astype(BF16)
+            o = (dot(exponent, v) / mass).astype(BF16)
             lifted = dot(o, lift_ref[h])
             out_ref[here, wide] = (ret[here, wide] + gate[here, h:h + 1] * lifted).astype(BF16)
-        return carry
-
-    share = blocks // PIECES
-
-    def attend_piece(p):
-        for n in range(p * share, (p + 1) * share):
-            attend(n, 0)
+
+    def attend(n):
+        attend_values(n, attend_keys(n))
+
+    def returned(kv, n):
+        for p in range(row_pieces):
+            if n * keys <= row_cuts[p] < (n + 1) * keys:
+                at = passes.rows(p)
+                kv_copy(kv, p).wait_recv()
+                acc = (acc_mk, acc_mv)[kv]
+                acc[at, :] += kv_in[kv, at, :].astype(F32)
 
     def load_waits():
         for i in range(2, len(pairs)):
@@ -476,7 +487,7 @@
         prepare(c, 0)
         retain(c)
 
-    early_parts = min(parts, -(-picks * share // per))
+    early_parts = min(parts, -(-picks // per))
 
     def in_tokens(p, distances):
         for d in distances:
@@ -495,27 +506,31 @@
             passes.relay(OUT, d, p)
 
     near, far = ins[:1], ins[1:]
+    last = blocks - 1
 
     @pl.when(is_edge)
     def _():
         in_tokens(0, near)
         in_tokens(1, near)
         pass_waits(0, early_parts)
-        build_piece(0)
+        build(0)
         passes.send_own(0)
         passes.share_own(0)
-        for p in range(half, PIECES):
+        for p in range(half + 1, PIECES):
             toks.send_own(p)
-        lend_all(late, lent)
+        lend_all(others, lent - 1)
         in_tokens(2, near)
         load_waits()
         tokens_of(IN, 0, 0)
         in_tokens(3, near)
         pass_waits(early_parts, parts)
-        for p in range(1, PIECES):
-            build_piece(p)
+        for n in range(1, blocks):
+            build(n)
+        for p in range(1, row_pieces):
             passes.send_own(p)
             passes.share_own(p)
+            if p == 1:
+                lend_all(lent - 1, lent)
         tokens_of(IN, 0, 1)
         in_tokens(0, ins[1:2])
         tokens_of(IN, 1, 0)
@@ -525,9 +540,10 @@
         tokens_of(IN, 2, 0)
         in_tokens(3, ins[1:2])
         tokens_of(IN, 2, 1)
-        for p in range(PIECES):
+        for p in range(row_pieces):
             rows_wait(p, 1)
-            rows_all(p, z * CORES, CORES)
+        for n in range(blocks):
+            rows_all(n, z * CORES, CORES)
         for d in ins[2:]:
             in_tokens(0, [d])
             in_tokens(1, [d])
@@ -540,12 +556,11 @@
             tokens_of(IN, d, 1)
         settle(2)
         settle(3)
-        for p in range(PIECES):
-            at = pl.ds(p * rows_piece, rows_piece)
-            for kv, acc in ((0, acc_mk), (1, acc_mv)):
-                kv_copy(kv, p).wait_recv()
-                acc[at, :] += kv_in[kv, at, :].astype(F32)
-            attend_piece(p)
+        for n in range(blocks):
+            returned(0, n)
+            state = attend_keys(n)
+            returned(1, n)
+            attend_values(n, state)
         lend_drain()
 
     @pl.when(depth > 0)
@@ -557,7 +572,7 @@
         in_tokens(2, near)
         spread_own(1, 2)
         pass_waits(0, early_parts)
-        build_piece(0)
+        build(0)
         passes.send_own(0)
         passes.share_own(0)
         in_tokens(3, near)
@@ -565,73 +580,79 @@
         load_waits()
         tokens_of(IN, 0, 0)
         in_tokens(0, far)
-        spread_own(2, 3)
+        spread_own(2, others)
         pass_waits(early_parts, parts)
-        for p in range(1, PIECES):
-            build_piece(p)
-            if p < PIECES - 1:
-                passes.send_own(p)
+        for n in range(1, blocks):
+            build(n)
+        for p in range(1, row_pieces):
             passes.share_own(p)
         tokens_of(IN, 0, 1)
+        out_tokens(2)
+        passes.send_own(1)
         in_rows(0, near)
-        spread_own(3, late)
         tokens_of(IN, 1, 0)
         in_tokens(1, far)
         out_rows(0)
         tokens_of(IN, 1, 1)
         for d in outs:
             tokens_of(OUT, d, 0)
-        out_tokens(2)
-        in_rows(1, near)
+        in_tokens(2, far)
+        out_tokens(3)
+        passes.send_own(2)
         spread_on(0, others - 1)
         for d in far:
             tokens_of(IN, d, 0)
-        out_tokens(3)
-        passes.send_own(PIECES - 1)
-        in_rows(2, near)
         spread_on(others - 1, others)
-        in_tokens(2, far)
-        spread_own(late, late + 1)
+        in_rows(1, near)
+        spread_own(others, lent - 2)
         settle(0)
         settle(1)
-        in_tokens(3, far)
-        spread_own(late + 1, lent)
-        spread_on(others, late)
-        for d in outs:
-            tokens_of(OUT, d, 1)
-        in_rows(3, near)
+        spread_own(lent - 2, lent - 1)
         in_rows(0, far)
         rows_wait(0, n_z)
         spread_last(0)
         assist(0, 0)
+        in_tokens(3, far)
         out_rows(1)
-        spread_on(late, late + 1)
+        for p in range(last, row_pieces):
+            passes.send_own(p)
+        spread_on(others, lent - 2)
+        for d in outs:
+            tokens_of(OUT, d, 1)
+        in_rows(2, near)
+        spread_own(lent - 1, lent)
+        spread_on(lent - 2, lent - 1)
         for d in far:
             tokens_of(IN, d, 1)
         out_rows(2)
-        spread_on(late + 1, lent)
+        in_rows(1, far)
+        settle(2)
+        spread_on(lent - 1, lent)
         out_rows(3)
-        in_rows(1, far)
         rows_wait(1, n_z)
         assist(0, 1)
+        out_rows(4)
+        in_rows(last, near)
         spread_last(1)
         assist(1, 0)
         assist(1, 1)
         in_rows(2, far)
-        settle(2)
+        settle(3)
+        in_rows(3, far)
         rows_wait(2, n_z)
         assist(0, 2)
         assist(1, 2)
-        settle(3)
-        in_rows(3, far)
-        rows_all(0, 0, n_tp)
+        in_rows(4, near)
+        in_rows(4, far)
         rows_wait(3, n_z)
         assist(0, 3)
         assist(1, 3)
-        attend_piece(0)
-        for p in range(1, PIECES):
-            rows_all(p, 0, n_tp)
-            attend_piece(p)
+        rows_wait(4, n_z)
+        assist(0, 4)
+        assist(1, 4)
+        for n in range(blocks):
+            rows_all(n, 0, n_tp)
+            attend(n)
 
         @pl.when(is_helper)
         def _():
@@ -678,8 +699,10 @@
         key_cols, mem_cols = w_query.shape[1], w_mem_query.shape[1]
         n_b = square_split(n_st)
 
-        def flow_sems(*pair_shape):
-            return dma((n_z, PIECES)), dma(pair_shape), dma((n_z,)), dma((1,)), dma((1,))
+        row_pieces = len(row_bounds(blocks, picks * pass_rows)) - 1
+
+        def flow_sems(pieces, *pair_shape):
+            return dma((n_z, pieces)), dma(pair_shape), dma((n_z,)), dma((1,)), dma((1,))
         all_rows = requests * pass_rows
         scratch = [
             V((n_tp, total, cols), BF16), V((n_tp, all_rows, cols), BF16),
@@ -688,7 +711,7 @@
             V(w_mem_query.shape, BF16), V(w_mem_key.shape, BF16), V(w_mem_value.shape, BF16),
             V(store.shape, BF16), V((n_st, cap, pass_rows, cols), BF16),
             tuple(V((n_st, cap // parts, pass_rows, cols), BF16) for _ in range(parts)),
-            V((n_st, picks, blocks), jnp.int32), pltpu.SMEM((n_st, picks, blocks), jnp.int32),
+            pltpu.SMEM((n_st, picks, blocks), jnp.int32),
             V((total, key_cols), F32), V((total, key_cols), F32), V((total, wide), F32), V((total, mem_cols), F32),
             V((total, heads), F32), V((total, 128), F32),
             V((all_rows, mem_cols), F32), V((all_rows, mem_cols), F32),
@@ -697,9 +720,9 @@
             V(w_mem_key.shape, BF16), V(w_mem_value.shape, BF16),
             V((2, all_rows, mem_cols), BF16), V((2, all_rows, mem_cols), BF16),
             dma((13,)), dma((n_st,)), dma((n_st,)), dma((1,)), dma((parts,)),
-            flow_sems(n_z, 2), flow_sems(PIECES),
+            flow_sems(PIECES, n_z, 2), flow_sems(row_pieces, row_pieces),
             dma((1,)), dma((2 * (n_z - 1),)), dma((2 * (n_z - 1), n_b - 1)), dma((2 * (n_z - 1), n_st // n_b - 1)),
-            dma((2,)), dma((2,)), dma((1,)), dma((2, PIECES)),
+            dma((2,)), dma((2,)), dma((1,)), dma((2, row_pieces)),
         ]
         return pl.pallas_call(
             functools.partial(kernel, n_st, n_tp, cap, picks, held),

time: 65.3 us -> 63.7 us (0.975)
  Pallas kernels: 64.3 us -> 62.7 us
    pallas_call x1, Pallas kernels: 64.3 us -> 62.7 us  [per_device(): pl.pallas_call(functools.partial(kernel, n_st, n_tp, cap, picks, held), o...]
where the time goes in v4:
time: 63.7 us; the launch traced here: 63.5 us
  Pallas kernels  62.7 us (98%)
  local copies, waits for them, and re-layouts  0.8 us (1%)
    pallas_call x1, Pallas kernels, per_device(): pl.pallas_call(functools.partial(kernel, n_st, n_tp, cap, picks, held), o...  62.7 us

profile of v4, /device:TPU:0, one launch (start us, length us, event | category | flops | bytes accessed | tf_op | source)
XLA Modules:
  0.0 63.5 jit_solution(16457687949307925547)
XLA Ops:
  0.0 62.7 %shard_map.136 = bf16[512,512]{1,0:T(8,128)(2,1)S(1)} custom-call(f32[2]{0:T(128)} %rate_ref.1, bf16[512,512]{1,0:T(8,128)(2,1)} %tok_hbm.1, bf16[4096,256]{1,0:T(8,128)(2,1)} %wq_hbm.1, bf16[4096,256]{1,0:T(8,128)(2,1)} %wk_hbm.1, bf16[4096,512]{1,0:T(8,128)(2,1)} %wv_hbm.1, bf16[4096,256]{1,0:T(8,128)(2,1)} %wm_hbm.1, bf16[4096,256]{1,0:T(8,128)(2,1)} %wmk_hbm.1, ...), custom_call_target="tpu_custom_call" | custom-call | tf_op jit(solution)/shard_map/pallas_call | solution.py:727
  62.7 0.8 %copy.16 = bf16[512,512]{1,0:T(8,128)(2,1)} copy(bf16[512,512]{1,0:T(8,128)(2,1)S(1)} %shard_map.136) | data formatting | bytes 1048576

commit v5 on v4

--- a/solution.py
+++ b/solution.py
@@ -644,13 +644,24 @@
         assist(1, 2)
         in_rows(4, near)
         in_rows(4, far)
-        rows_wait(3, n_z)
-        assist(0, 3)
-        assist(1, 3)
-        rows_wait(4, n_z)
-        assist(0, 4)
-        assist(1, 4)
-        for n in range(blocks):
+
+        def last_returns():
+            for p in range(last, row_pieces):
+                rows_wait(p, n_z)
+                assist(0, p)
+                assist(1, p)
+
+        @pl.when(core == 0)
+        def _():
+            last_returns()
+        for n in range(blocks // 2):
+            rows_all(n, 0, n_tp)
+            attend(n)
+
+        @pl.when(core > 0)
+        def _():
+            last_returns()
+        for n in range(blocks // 2, blocks):
             rows_all(n, 0, n_tp)
             attend(n)
 

time: 63.7 us -> 63.1 us (level)
  no operation moved by 1% of the time
where the time goes in v5:
time: 63.1 us; the launch traced here: 62.9 us
  Pallas kernels  62.1 us (98%)
  local copies, waits for them, and re-layouts  0.8 us (1%)
    pallas_call x1, Pallas kernels, per_device(): pl.pallas_call(functools.partial(kernel, n_st, n_tp, cap, picks, held), o...  62.1 us

profile of v5, /device:TPU:0, one launch (start us, length us, event | category | flops | bytes accessed | tf_op | source)
XLA Modules:
  0.0 62.9 jit_solution(16260542053422474075)
XLA Ops:
  0.0 62.1 %shard_map.136 = bf16[512,512]{1,0:T(8,128)(2,1)S(1)} custom-call(f32[2]{0:T(128)} %rate_ref.1, bf16[512,512]{1,0:T(8,128)(2,1)} %tok_hbm.1, bf16[4096,256]{1,0:T(8,128)(2,1)} %wq_hbm.1, bf16[4096,256]{1,0:T(8,128)(2,1)} %wk_hbm.1, bf16[4096,512]{1,0:T(8,128)(2,1)} %wv_hbm.1, bf16[4096,256]{1,0:T(8,128)(2,1)} %wm_hbm.1, bf16[4096,256]{1,0:T(8,128)(2,1)} %wmk_hbm.1, ...), custom_call_target="tpu_custom_call" | custom-call | tf_op jit(solution)/shard_map/pallas_call | solution.py:738
  62.1 0.8 %copy.16 = bf16[512,512]{1,0:T(8,128)(2,1)} copy(bf16[512,512]{1,0:T(8,128)(2,1)S(1)} %shard_map.136) | data formatting | bytes 1048576
